TPU v7x, 512 devices: a whole 4x8x8 slice. The times are simulated.
512 devices in a mesh: sp: 64 (over z, y), tp: 8 (over x, core).
Axes of the slice: x: 4, y: 8, z: 8, core: 2. Of those that a mesh axis runs over, the one named last changes fastest.
Arguments:
- target: bfloat16 [16384, 1024], P(('sp', 'tp')), may hold values from -60 to 60
- source: bfloat16 [8192, 1024], P('sp'), may hold values from -7 to 7
- target_gains: bfloat16 [2, 4, 1024], replicated, may hold values from 0.099609375 to 1.8984375
- source_gain: bfloat16 [2, 1024], replicated, may hold values from 0.099609375 to 1.8984375
- query_weight: bfloat16 [2, 1024, 1024], P(None, None, 'tp'), may hold values from -0.1875 to 0.1875
- key_weight: bfloat16 [2, 1024, 1024], P(None, None, 'tp'), may hold values from -7.5625 to 7.5625
- value_weight: bfloat16 [2, 1024, 1024], P(None, None, 'tp'), may hold values from -0.1875 to 0.1875
- out_weight: bfloat16 [2, 1024, 1024], P(None, 'tp'), may hold values from -0.1875 to 0.1875
- gate_weight: bfloat16 [2, 1024, 1536], P(None, None, 'tp'), may hold values from -0.1875 to 0.1875
- up_weight: bfloat16 [2, 1024, 1536], P(None, None, 'tp'), may hold values from -0.1875 to 0.1875
- down_weight: bfloat16 [2, 1536, 1024], P(None, 'tp'), may hold values from -0.15625 to 0.15625
Outputs:
- stream: bfloat16 [16384, 1024], P(('sp', 'tp'))
All inputs are finite; a program needn't handle non-finite values.
Results may differ from a plain program's by a relative error of at most 0.04.
Values may be sent and summed in bfloat16 or wider, within the bound.
A program may use at most 64 MiB of HBM per device.

v0:
```python
import jax
import jax.numpy as jnp
from jax import lax
from jax.sharding import PartitionSpec as P

HEAD_DIM = 128


epsilon = 1e-06


def sent_to_all(shard, axis):
    copies = jnp.broadcast_to(shard, (lax.axis_size(axis), *shard.shape))
    return lax.all_to_all(copies, axis, split_axis=0, concat_axis=0, tiled=True)


def joined_along(blocks, dim):
    lengths = list(blocks.shape[1:])
    lengths[dim] *= blocks.shape[0]
    return jnp.moveaxis(blocks, 0, dim).reshape(lengths)


def collect(shard, axis, dim):
    blocks = sent_to_all(shard, axis)
    return joined_along(blocks, dim)


def in_one_piece(arrays, axis, dim, along):
    widths = [a.shape[along] for a in arrays]
    both = jnp.concatenate(arrays, axis=along)
    result = lax.all_gather(both, axis, axis=dim, tiled=True)
    return tuple(jnp.split(result, [sum(widths[:k]) for k in range(1, len(widths))], axis=along))


def in_blocks(shard, dim, count):
    before, after = (shard.shape[:dim], shard.shape[dim + 1 :])
    return jnp.moveaxis(shard.reshape(*before, count, -1, *after), dim, 0)


def sent_and_summed(shard, axis, dim):
    blocks = in_blocks(shard, dim, lax.axis_size(axis))
    arrived = lax.all_to_all(blocks, axis, split_axis=0, concat_axis=0, tiled=True)
    return arrived.astype(jnp.float32).sum(axis=0)


def rms_norm(values, gain_row):
    widened = values.astype(jnp.float32)
    inverse = lax.rsqrt(jnp.mean(widened * widened, axis=-1, keepdims=True) + epsilon)
    return widened * inverse * gain_row.astype(jnp.float32)


def per_device(
    target,
    source,
    target_gains,
    source_gain,
    query_weight,
    key_weight,
    value_weight,
    out_weight,
    gate_weight,
    up_weight,
    down_weight,
):
    layers = query_weight.shape[0]
    own_rows = target.shape[0]
    heads_dev = query_weight.shape[2] // HEAD_DIM
    factor = HEAD_DIM ** (-0.5)
    stream = target
    for layer_index in range(layers):
        layer_gains = target_gains[layer_index]
        normed = rms_norm(stream, layer_gains[0]).astype(jnp.bfloat16)

        def query_piece(row_piece, offset, layer_index=layer_index):
            return jnp.dot(
                row_piece, query_weight[layer_index], preferred_element_type=jnp.float32
            ).astype(jnp.bfloat16)

        queries = query_piece(collect(normed, "tp", 0), jnp.int32(0))
        group_rows = queries.shape[0]
        query_heads = queries.reshape(group_rows, heads_dev, HEAD_DIM)

        def attend(folded, pieces, offset, query_heads=query_heads):
            running_max, running_sum, weighted = folded
            key_heads = pieces[0].reshape(pieces[0].shape[0], heads_dev, HEAD_DIM)
            value_heads = pieces[1].reshape(pieces[1].shape[0], heads_dev, HEAD_DIM)
            scores = (
                jnp.einsum(
                    "thd,shd->ths", query_heads, key_heads, preferred_element_type=jnp.float32
                )
                * factor
            )
            new_max = jnp.maximum(running_max, jnp.max(scores, axis=-1))
            weights = jnp.exp(scores - new_max[..., None])
            running_sum = jnp.sum(weights, axis=-1)
            weighted = jnp.einsum(
                "ths,shd->thd",
                weights.astype(jnp.bfloat16),
                value_heads,
                preferred_element_type=jnp.float32,
            )
            return (new_max, running_sum, weighted)

        initial = (
            jnp.full((group_rows, heads_dev), -1e30, jnp.float32),
            jnp.zeros((group_rows, heads_dev), jnp.float32),
            jnp.zeros((group_rows, heads_dev, HEAD_DIM), jnp.float32),
        )
        normed_source = rms_norm(source, source_gain[layer_index]).astype(jnp.bfloat16)
        key_rows = jnp.dot(
            normed_source, key_weight[layer_index], preferred_element_type=jnp.float32
        ).astype(jnp.bfloat16)
        value_rows = jnp.dot(
            normed_source, value_weight[layer_index], preferred_element_type=jnp.float32
        ).astype(jnp.bfloat16)
        key_rows, value_rows = (key_rows, value_rows)
        folded = attend(initial, in_one_piece((key_rows, value_rows), "sp", 0, 1), jnp.int32(0))
        running_max, running_sum, weighted = folded
        context = (
            (weighted / running_sum[..., None])
            .reshape(group_rows, heads_dev * HEAD_DIM)
            .astype(jnp.bfloat16)
        )

        def attn_term(offset, length, layer_index=layer_index, context=context):
            return jnp.dot(context, out_weight[layer_index], preferred_element_type=jnp.float32)

        attended = sent_and_summed(
            attn_term(jnp.int32(0), own_rows * lax.axis_size("tp")).astype(jnp.bfloat16), "tp", 0
        ).astype(jnp.bfloat16)
        stream = (stream.astype(jnp.float32) + rms_norm(attended, layer_gains[1])).astype(
            jnp.bfloat16
        )
        mixer_in = rms_norm(stream, layer_gains[2]).astype(jnp.bfloat16)

        def mixer_piece(row_piece, offset, layer_index=layer_index):
            gate_part = jnp.dot(
                row_piece, gate_weight[layer_index], preferred_element_type=jnp.float32
            )
            up_part = jnp.dot(row_piece, up_weight[layer_index], preferred_element_type=jnp.float32)
            return (jax.nn.silu(gate_part) * up_part).astype(jnp.bfloat16)

        hidden = mixer_piece(collect(mixer_in, "tp", 0), jnp.int32(0))

        def mixer_term(offset, length, layer_index=layer_index, hidden=hidden):
            return jnp.dot(hidden, down_weight[layer_index], preferred_element_type=jnp.float32)

        mixer_out = sent_and_summed(
            mixer_term(jnp.int32(0), own_rows * lax.axis_size("tp")).astype(jnp.bfloat16), "tp", 0
        ).astype(jnp.bfloat16)
        stream = (stream.astype(jnp.float32) + rms_norm(mixer_out, layer_gains[3])).astype(
            jnp.bfloat16
        )
    return stream


def solution(mesh):
    placed = (
        P(("sp", "tp"), None),
        P("sp", None),
        P(),
        P(),
        P(None, None, "tp"),
        P(None, None, "tp"),
        P(None, None, "tp"),
        P(None, "tp", None),
        P(None, None, "tp"),
        P(None, None, "tp"),
        P(None, "tp", None),
    )
    return jax.shard_map(
        per_device, mesh=mesh, in_specs=placed, out_specs=P(("sp", "tp"), None), check_vma=False
    )
```

profile of v0, /device:TPU:1, one launch (start us, length us, event | category | flops | bytes accessed | tf_op | source)
XLA Modules:
  0.0 267.0 jit_solution(10817497825534002607)
XLA Ops:
  6.5 1.1 fusion.72
  7.6 0.8 slice_convert_fusion.9
  8.4 1.4 convolution_convert_fusion.8
  9.8 1.4 convolution_convert_fusion.9
  11.1 0.6 pad_maximum_fusion
  11.8 1.3 convolution_convert_fusion.6
  13.2 1.4 convolution_convert_fusion.7
  14.5 0.6 pad_maximum_fusion.1
  15.2 1.0 fusion.129
  16.2 0.9 slice_convert_fusion
  17.1 0.9 fusion.131
  18.0 0.1 broadcast_in_dim.8
  18.1 18.6 %all_to_all.40 = bf16[8,32,1024]{2,1,0:T(8,128)(2,1)S(1)} all-to-all(bf16[8,32,1024]{2,1,0:T(8,128)(2,1)S(1)} %broadcast_in_dim.8), channel_id=1, replica_groups=mesh['sp'=64,'tp'=8] {'tp'}, dimensions={0} | all-to-all | bytes 1048576 | tf_op jit(solution)/shard_map/all_to_all | solution.py:14
  36.6 67.9 %all-gather.3.cloned.1.call-done = bf16[8192,256]{0,1:T(8,128)(2,1)} async-done(((bf16[128,256]{0,1:T(8,128)(2,1)}), bf16[8192,256]{0,1:T(8,128)(2,1)}) %all-gather.3.cloned.1.call-update) | async-done | bytes 4194320 | tf_op jit(solution)/shard_map/all_gather | solution.py:31
  104.6 6.6 %fusion.158 = (f32[256]{0:T(256)S(1)}, f32[8192,256]{1,0:T(8,128)}) fusion(bf16[256,1024]{1,0:T(8,128)(2,1)S(1)} %bitcast.179, bf16[2,1024,128]{2,1,0:T(8,128)(2,1)} %param.15, bf16[8192,256]{0,1:T(8,128)(2,1)} %all-gather.3.cloned.1.call-done), kind=kOutput, calls=%fused_computation.162 | convolution fusion | flops 608206592 | bytes 11273216 | tf_op jit(solution)/shard_map/thd,shd->ths/dot_general | solution.py:88
  111.2 4.6 %fusion.2 = f32[256]{0:T(256)S(1)} fusion(f32[8192,256]{1,0:T(8,128)} %get-tuple-element.22, f32[256]{0:T(256)S(1)} %broadcast_maximum_fusion.1), kind=kLoop, calls=%fused_computation.6 | loop fusion | flops 4194048 | bytes 8390656 | tf_op jit(solution)/shard_map/reduce_sum | solution.py:95
  115.8 6.0 %convolution_convert_fusion.3 = bf16[256,1024]{1,0:T(8,128)(2,1)S(1)} fusion(f32[8192,256]{1,0:T(8,128)} %get-tuple-element.22, f32[256]{0:T(256)S(1)} %broadcast_maximum_fusion.1, bf16[8192,256]{0,1:T(8,128)(2,1)} %all-gather.3.cloned.1.call-done, bf16[2,128,1024]{2,1,0:T(8,128)(2,1)S(1)} %copy-done.3, f32[256]{0:T(256)S(1)} %fusion.2), kind=kOutput, calls=%fused_computation.23 | convolution fusion | flops 608501760 | bytes 11274240 | tf_op jit(solution)/shard_map/dot_general | solution.py:126
  121.8 18.9 %all_to_all.41 = bf16[8,32,1024]{2,1,0:T(8,128)(2,1)S(1)} all-to-all(bf16[8,32,1024]{2,1,0:T(8,128)(2,1)S(1)} %bitcast.180), channel_id=1, replica_groups=mesh['sp'=64,'tp'=8] {'tp'}, dimensions={0} | all-to-all | bytes 1048576 | tf_op jit(solution)/shard_map/all_to_all | solution.py:42
  140.7 0.1 reduce_sum.154
  140.8 0.1 fusion.121
  140.9 0.2 fusion.133
  141.1 0.1 fusion.135
  141.3 12.8 %all_to_all.42 = bf16[8,32,1024]{2,1,0:T(8,128)(2,1)S(1)} all-to-all(bf16[8,32,1024]{2,1,0:T(8,128)(2,1)S(1)} %broadcast_in_dim.9), channel_id=1, replica_groups=mesh['sp'=64,'tp'=8] {'tp'}, dimensions={0} | all-to-all | bytes 1048576 | tf_op jit(solution)/shard_map/all_to_all | solution.py:14
  154.0 0.3 fusion.81
  154.4 2.0 convolution_convert_fusion.1
  156.4 12.8 %all_to_all.43 = bf16[8,32,1024]{2,1,0:T(8,128)(2,1)S(1)} all-to-all(bf16[8,32,1024]{2,1,0:T(8,128)(2,1)S(1)} %bitcast.186), channel_id=1, replica_groups=mesh['sp'=64,'tp'=8] {'tp'}, dimensions={0} | all-to-all | bytes 1048576 | tf_op jit(solution)/shard_map/all_to_all | solution.py:42
  169.1 0.1 reduce_sum.157
  169.2 0.1 fusion.123
  169.4 0.2 fusion.137
  169.6 0.1 fusion.139
  169.7 0.8 broadcast_in_dim.10
  170.5 4.4 %all-to-all-start.4 = ((bf16[8,32,1024]{2,1,0:T(8,128)(2,1)}), bf16[8,32,1024]{2,1,0:T(8,128)(2,1)S(1)}, u32[]{:S(2)}, u32[]{:S(2)}) async-start(bf16[8,32,1024]{2,1,0:T(8,128)(2,1)} %broadcast_in_dim.10), calls=%async_computation.4 | async-start | bytes 1048576 | tf_op jit(solution)/shard_map/all_to_all | solution.py:14
  175.0 19.5 %all-gather.5.cloned.1.call-done = bf16[8192,256]{0,1:T(8,128)(2,1)} async-done(((bf16[128,256]{0,1:T(8,128)(2,1)}), bf16[8192,256]{0,1:T(8,128)(2,1)}) %all-gather.5.cloned.1.call-update) | async-done | bytes 4194320 | tf_op jit(solution)/shard_map/all_gather | solution.py:31
  194.5 6.6 %fusion.161 = (f32[256]{0:T(256)S(1)}, f32[8192,256]{1,0:T(8,128)}) fusion(bf16[256,1024]{1,0:T(8,128)(2,1)S(1)} %bitcast.178, bf16[2,1024,128]{2,1,0:T(8,128)(2,1)S(1)} %copy-done.2, bf16[8192,256]{0,1:T(8,128)(2,1)} %all-gather.5.cloned.1.call-done), kind=kOutput, calls=%fused_computation.163 | convolution fusion | flops 608206592 | bytes 11273216 | tf_op jit(solution)/shard_map/thd,shd->ths/dot_general | solution.py:88
  201.0 4.5 %fusion.4 = f32[256]{0:T(256)S(1)} fusion(f32[8192,256]{1,0:T(8,128)} %get-tuple-element.24, f32[256]{0:T(256)S(1)} %broadcast_maximum_fusion), kind=kLoop, calls=%fused_computation.8 | loop fusion | flops 4194048 | bytes 8390656 | tf_op jit(solution)/shard_map/reduce_sum | solution.py:95
  205.6 5.9 %convolution_convert_fusion.2 = bf16[256,1024]{1,0:T(8,128)(2,1)S(1)} fusion(f32[8192,256]{1,0:T(8,128)} %get-tuple-element.24, f32[256]{0:T(256)S(1)} %broadcast_maximum_fusion, bf16[8192,256]{0,1:T(8,128)(2,1)} %all-gather.5.cloned.1.call-done, bf16[2,128,1024]{2,1,0:T(8,128)(2,1)S(1)} %copy-done.3, f32[256]{0:T(256)S(1)} %fusion.4), kind=kOutput, calls=%fused_computation.22 | convolution fusion | flops 608501760 | bytes 11274240 | tf_op jit(solution)/shard_map/dot_general | solution.py:126
  211.5 19.2 %all_to_all.44 = bf16[8,32,1024]{2,1,0:T(8,128)(2,1)S(1)} all-to-all(bf16[8,32,1024]{2,1,0:T(8,128)(2,1)S(1)} %bitcast.181), channel_id=1, replica_groups=mesh['sp'=64,'tp'=8] {'tp'}, dimensions={0} | all-to-all | bytes 1048576 | tf_op jit(solution)/shard_map/all_to_all | solution.py:42
  230.7 0.1 reduce_sum.161
  230.8 0.1 fusion.125
  230.9 0.2 fusion.141
  231.2 0.1 fusion.143
  231.3 12.8 %all_to_all.45 = bf16[8,32,1024]{2,1,0:T(8,128)(2,1)S(1)} all-to-all(bf16[8,32,1024]{2,1,0:T(8,128)(2,1)S(1)} %broadcast_in_dim.11), channel_id=1, replica_groups=mesh['sp'=64,'tp'=8] {'tp'}, dimensions={0} | all-to-all | bytes 1048576 | tf_op jit(solution)/shard_map/all_to_all | solution.py:14
  244.1 0.3 fusion.76
  244.4 2.0 convolution_convert_fusion
  246.4 12.8 %all_to_all.46 = bf16[8,32,1024]{2,1,0:T(8,128)(2,1)S(1)} all-to-all(bf16[8,32,1024]{2,1,0:T(8,128)(2,1)S(1)} %bitcast.187), channel_id=1, replica_groups=mesh['sp'=64,'tp'=8] {'tp'}, dimensions={0} | all-to-all | bytes 1048576 | tf_op jit(solution)/shard_map/all_to_all | solution.py:42
  259.2 0.1 reduce_sum.164
  259.3 0.1 fusion.127
  259.4 0.7 fusion.144
  (26 shorter events, 0.3 us)
Async XLA Ops:
  6.5 98.0 %all-gather.3.cloned.1.call-start = ((), (), s32[]{:S(2)}) async-start(), calls=%async_computation.8 | async-start | bytes 4259840 | tf_op jit(solution)/shard_map/all_gather | solution.py:31
  11.8 182.7 %all-gather.5.cloned.1.call-start = ((), (), s32[]{:S(2)}) async-start(), calls=%async_computation.9 | async-start | bytes 4259840 | tf_op jit(solution)/shard_map/all_gather | solution.py:31
  104.6 11.2 %copy-start.3 = (bf16[2,128,1024]{2,1,0:T(8,128)(2,1)S(1)}, bf16[2,128,1024]{2,1,0:T(8,128)(2,1)}, u32[]{:S(2)}) copy-start(bf16[2,128,1024]{2,1,0:T(8,128)(2,1)} %param.18) | copy-start | bytes 1572868
  115.8 25.1 %copy-start.1 = (bf16[32,1024]{1,0:T(8,128)(2,1)S(1)}, bf16[32,1024]{1,0:T(8,128)(2,1)}, u32[]{:S(2)}) copy-start(bf16[32,1024]{1,0:T(8,128)(2,1)} %param.11) | copy-start | bytes 196612
  115.8 38.3 %copy-start = (bf16[2,1024,192]{1,2,0:T(8,128)(2,1)S(1)}, bf16[2,1024,192]{1,2,0:T(8,128)(2,1)}, u32[]{:S(2)}) copy-start(bf16[2,1024,192]{1,2,0:T(8,128)(2,1)} %param.19) | copy-start | bytes 2359300
  121.8 72.7 %copy-start.2 = (bf16[2,1024,128]{2,1,0:T(8,128)(2,1)S(1)}, bf16[2,1024,128]{2,1,0:T(8,128)(2,1)}, u32[]{:S(2)}) copy-start(bf16[2,1024,128]{2,1,0:T(8,128)(2,1)} %param.15) | copy-start | bytes 1572868
  170.5 23.9 %all-to-all-start.4 = ((bf16[8,32,1024]{2,1,0:T(8,128)(2,1)}), bf16[8,32,1024]{2,1,0:T(8,128)(2,1)S(1)}, u32[]{:S(2)}, u32[]{:S(2)}) async-start(bf16[8,32,1024]{2,1,0:T(8,128)(2,1)} %broadcast_in_dim.10), calls=%async_computation.4 | async-start | bytes 1048576 | tf_op jit(solution)/shard_map/all_to_all | solution.py:14
Sparse Core Ops, SparseCore 0:
  11.9 92.6 all-gather.2
  107.5 86.8 all-gather.4
where the time goes:
time: 268 us; the launch traced here: 267 us
  blocking collectives  108 us (40%)
  waiting for transfers between devices  87.5 us (33%)
  matrix products  35.2 us (13%)
  other arithmetic  17.6 us (7%)
  between operations  13.6 us (5%)
  starting transfers between devices  4.48 us (2%)
    all_gather x2, waiting for transfers between devices, in_one_piece(): result = lax.all_gather(both, axis, axis=dim, tiled=True)  87.4 us
    all_to_all x4, blocking collectives, sent_and_summed(): lax.all_to_all(blocks, axis, split_axis=0, concat_axis=0, tiled=True)  63.6 us
    all_to_all x3, blocking collectives, sent_to_all(): return lax.all_to_all(copies, axis, split_axis=0, concat_axis=0, tiled=True)  44.1 us
    dot_general x2, matrix products, attend(): jnp.einsum('thd,shd->ths', query_heads, key_heads, preferred_element_type...  13.2 us
    dot_general x2, matrix products, attn_term(): jnp.dot(context, out_weight[layer_index], preferred_element_type=jnp.floa...  11.9 us
    reduce_sum x2, other arithmetic, attend(): running_sum = jnp.sum(weights, axis=-1)  9.1 us
  transfers between devices with their start and end apart: 3, of which 2 were waited for; matrix products, arithmetic and copies ran while one was open for 10% of the time, Pallas kernels for 0%

commit v1 on v0

v1 whole, which is shorter than its diff:
```python
import functools
import math

import jax
import jax.numpy as jnp
from jax import lax
from jax.experimental import pallas as pl
from jax.experimental.pallas import tpu as pltpu
from jax.sharding import PartitionSpec as P

MESH = pl.DeviceIdType.MESH
BF = jnp.bfloat16
F32 = jnp.float32
EPS = 1e-06
HD = 128
D = 1024
ROWS = 32
GROUP = 128
BLOCKS = 64
LAYERS = 2
STEPS = 8 * LAYERS
QSCALE = HD ** (-0.5) * math.log2(math.e)


def rms(v, gain):
    inverse = lax.rsqrt(jnp.mean(v * v, axis=-1, keepdims=True) + EPS)
    return v * inverse * gain


def dot(a, b):
    return jnp.dot(a, b, preferred_element_type=F32)


def ring_offset(k):
    return ((k + 1) // 2) * (2 * (k % 2) - 1)


def kernel(
    target, source, tgains, sgain, qw_in, kw_in, vw_in, ow_in, gw_in, uw_in, dw_in,
    out,
    src_v, tg_v, sg_v, kw, vw, qw, gw, uw, dw, ow,
    kv, xg, qown, qrecv, qsend, cx, csend, mid, rsend, rs,
    m_ref, l_ref, acc_ref,
    r2, r1, kvs, loc, wts, own_sem, x_recv, x_send, q_recv, q_send, c_recv, c_send, s_recv, s_send,
    pw_recv, pw_send, o_recv, o_send, of_recv, of_send,
):
    sp = lax.axis_index("sp")
    tp = lax.axis_index("tp")
    c = lax.rem(tp, 2)
    x = tp // 2
    z_pos, y_pos = sp // 8, lax.rem(sp, 8)
    f = (1 - c) * y_pos + c * z_pos
    s = (1 - c) * z_pos + c * y_pos

    def sp_of(fp, spos):
        return fp * (1 + 7 * c) + spos * (8 - 7 * c)

    def wrap(v):
        return lax.rem(v + 16, 8)

    ring1 = (sp_of(wrap(f + 1), s), sp_of(wrap(f - 1), s))
    ring2 = (sp_of(f, wrap(s + 1)), sp_of(f, wrap(s - 1)))
    partner = x * 2 + (1 - c)

    def other_x(k):
        return lax.rem(x + k, 4)

    def local(src, dst, sem):
        copy = pltpu.make_async_copy(src, dst, sem)
        copy.start()
        return copy

    first = [
        local(source, src_v, loc.at[0]),
        local(kw_in, kw, loc.at[1]),
        local(vw_in, vw, loc.at[2]),
        local(sgain, sg_v, loc.at[3]),
    ]
    target_load = local(target, xg.at[0, x], loc.at[4])
    gains_load = local(tgains, tg_v, loc.at[5])
    q_load = local(qw_in, qw.at[c], loc.at[6])
    late = [
        local(gw_in, gw.at[c], wts.at[0]),
        local(uw_in, uw.at[c], wts.at[1]),
        local(dw_in, dw.at[c], wts.at[2]),
    ]
    own_rows = pl.ds(pl.multiple_of((c * 4 + x) * HD, HD), HD)
    own_out = [
        local(ow_in.at[l], ow.at[l, own_rows], own_sem.at[l]) for l in range(LAYERS)
    ]

    barrier = pltpu.get_barrier_semaphore()
    peers = [(ring1[0], tp), (ring1[1], tp), (ring2[0], tp), (ring2[1], tp)]
    peers += [(sp, lax.rem(tp + k, 8)) for k in range(1, 8)]
    for peer in peers:
        pl.semaphore_signal(barrier, inc=1, device_id=peer, device_id_type=MESH)
    pl.semaphore_wait(barrier, len(peers))

    def remote(src, dst, send, recv, device):
        pltpu.make_async_remote_copy(
            src_ref=src, dst_ref=dst, send_sem=send, recv_sem=recv,
            device_id=device, device_id_type=MESH,
        ).start()

    def await_bytes(ref, sem):
        pltpu.make_async_copy(ref, ref, sem).wait()

    target_load.wait()
    for k in (2, 1, 3):
        remote(xg.at[0, x], xg.at[0, x], x_send.at[0], x_recv.at[0], (sp, other_x(k) * 2 + c))
    for i, (w_in, buf) in enumerate(((qw_in, qw), (gw_in, gw), (uw_in, uw), (dw_in, dw))):
        remote(w_in, buf.at[c], pw_send.at[i], pw_recv.at[i], (sp, partner))
    for l in range(LAYERS):
        for k in (2, 1, 3):
            remote(
                ow_in.at[l], ow.at[l, own_rows], o_send.at[l], o_recv.at[l],
                (sp, other_x(k) * 2 + c),
            )

    def slot_of(fp, spos):
        return fp * 8 + spos

    for copy in first:
        copy.wait()
    wide = src_v[...].astype(F32)
    scaled = wide * lax.rsqrt(jnp.mean(wide * wide, axis=-1, keepdims=True) + EPS)
    source_gains = sg_v[...].astype(F32)

    def project_source(l):
        normed = (scaled * source_gains[l : l + 1]).astype(BF)
        kv[l, slot_of(f, s), 0] = dot(normed, kw[l]).astype(BF)
        kv[l, slot_of(f, s), 1] = jnp.transpose(dot(normed, vw[l])).astype(BF)

    def send1(l, hop, way):
        delta = hop - 1
        fp = wrap(f - delta) if way == 0 else wrap(f + delta)
        block = kv.at[l, slot_of(fp, s)]
        if hop == 4:
            block = block.at[way]
        remote(block, block, kvs.at[l], r1.at[l, hop - 1, way], (ring1[way], tp))

    def recv1(l, hop, way):
        fp = wrap(f - hop) if way == 0 else wrap(f + hop)
        block = kv.at[l, slot_of(fp, s)]
        if hop == 4:
            block = block.at[way]
        await_bytes(block, r1.at[l, hop - 1, way])

    def send2(n, hop, way):
        l, k = divmod(n, 8)
        fp = wrap(f + ring_offset(k))
        delta = hop - 1
        spos = wrap(s - delta) if way == 0 else wrap(s + delta)
        block = kv.at[l, slot_of(fp, spos)]
        if hop == 4:
            block = block.at[way]
        remote(block, block, kvs.at[l], r2.at[n, hop - 1, way], (ring2[way], tp))

    def recv2(n, hop, way):
        l, k = divmod(n, 8)
        fp = wrap(f + ring_offset(k))
        spos = wrap(s - hop) if way == 0 else wrap(s + hop)
        block = kv.at[l, slot_of(fp, spos)]
        if hop == 4:
            block = block.at[way]
        await_bytes(block, r2.at[n, hop - 1, way])

    def ring_step(m):
        for l in range(LAYERS):
            hop = m - 4 * l
            if hop == 0:
                for way in (0, 1):
                    send1(l, 1, way)
            elif 1 <= hop <= 4:
                for way in (1, 0):
                    recv1(l, hop, way)
                    if hop < 4:
                        send1(l, hop + 1, way)
        if m < STEPS:
            for way in (0, 1):
                send2(m, 1, way)
        for hop in (1, 2, 3, 4):
            n = m - hop
            if 0 <= n < STEPS:
                for way in (0, 1):
                    recv2(n, hop, way)
                    if hop < 4:
                        send2(n, hop + 1, way)

    def attend(m, l):
        low = max(1, m - (8 * l + 7))
        high = min(4, m - 8 * l)
        if low > high:
            return

        def body(hop, carry):
            k = m - hop - 8 * l
            fp = wrap(f + ring_offset(k))
            left = slot_of(fp, wrap(s - lax.rem(hop, 4)))
            right = slot_of(fp, wrap(s + hop))
            queries = qcat(l)
            key_pair = jnp.concatenate([kv[l, left, 0], kv[l, right, 0]], axis=0)
            value_pair = jnp.concatenate([kv[l, left, 1], kv[l, right, 1]], axis=1)
            scores = dot(key_pair, queries)
            old = m_ref[...]
            new = jnp.maximum(old, jnp.max(scores, axis=0, keepdims=True))
            shrink = jnp.exp2(old - new)
            weights = jnp.exp2(scores - new)
            m_ref[...] = new
            l_ref[...] = l_ref[...] * shrink + jnp.sum(weights, axis=0, keepdims=True)
            acc_ref[...] = acc_ref[...] * shrink + dot(value_pair, weights.astype(BF))
            return carry

        lax.fori_loop(low, high + 1, body, 0)

    def qcat(l):
        return jnp.concatenate([qown[l], qrecv[l]], axis=1)

    def start_queries(l):
        gain = tg_v[l].astype(F32)[0:1]
        rows = xg[l].reshape(GROUP, D).astype(F32)
        normed = rms(rows, gain).astype(BF)
        theirs = dot(normed, qw[1 - c, l]) * QSCALE
        qsend[l] = jnp.transpose(theirs).astype(BF)
        remote(qsend.at[l], qrecv.at[l], q_send.at[l], q_recv.at[l], (sp, partner))
        mine = dot(normed, qw[c, l]) * QSCALE
        qown[l] = jnp.transpose(mine).astype(BF)
        m_ref[...] = jnp.full_like(m_ref, -1e30)
        l_ref[...] = jnp.zeros_like(l_ref)
        acc_ref[...] = jnp.zeros_like(acc_ref)

    def await_queries(l):
        await_bytes(qrecv.at[l], q_recv.at[l])

    def send_context(l):
        context = jnp.transpose(acc_ref[...] / l_ref[...]).astype(BF)
        slot = c * 4 + x
        csend[l] = context
        for k in (2, 1, 3):
            remote(
                csend.at[l, pl.ds(0, GROUP)], cx.at[l, slot], c_send.at[l], c_recv.at[l],
                (sp, other_x(k) * 2 + c),
            )
            remote(
                csend.at[l, pl.ds(GROUP, GROUP)], cx.at[l, slot], c_send.at[l], c_recv.at[l],
                (sp, other_x(k) * 2 + 1 - c),
            )
        remote(
            csend.at[l, pl.ds(GROUP, GROUP)], cx.at[l, slot], c_send.at[l], c_recv.at[l],
            (sp, partner),
        )
        cx[l, slot] = context[:GROUP]

    def after_context(l):
        await_bytes(cx.at[l, pl.ds(0, 7)], c_recv.at[l])
        gains = tg_v[l].astype(F32)
        contexts = jnp.concatenate([cx[l, j] for j in range(8)], axis=1)
        attended = dot(contexts, ow[l]).astype(BF).astype(F32)
        rows = xg[l].reshape(GROUP, D).astype(F32)
        stream = (rows + rms(attended, gains[1:2])).astype(BF)
        mid[l] = stream
        mixer_in = rms(stream.astype(F32), gains[2:3]).astype(BF)
        mixed = None
        for j in range(2):
            gate = dot(mixer_in, gw[j, l])
            up = dot(mixer_in, uw[j, l])
            hidden = (gate / (1.0 + jnp.exp(-gate)) * up).astype(BF)
            term = dot(hidden, dw[j, l])
            mixed = term if mixed is None else mixed + term
        rsend[l] = mixed.astype(BF).reshape(4, ROWS, D)
        for k in (2, 1, 3):
            remote(
                rsend.at[l, other_x(k)], rs.at[l, x], s_send.at[l], s_recv.at[l],
                (sp, other_x(k) * 2 + c),
            )
        rs[l, x] = rsend[l, x]

    def after_sum(l):
        await_bytes(rs.at[l, pl.ds(0, 3)], s_recv.at[l])
        gain = tg_v[l].astype(F32)[3:4]
        total = rs[l, 0].astype(F32)
        for j in range(1, 4):
            total = total + rs[l, j].astype(F32)
        mixer_out = total.astype(BF).astype(F32)
        own = mid[l, pl.ds(pl.multiple_of(x * ROWS, ROWS), ROWS)].astype(F32)
        return (own + rms(mixer_out, gain)).astype(BF)

    def forward_out(l):
        for k in range(1):
            own_out[l].wait()
        await_bytes(ow.at[l, pl.ds(0, 3 * HD)], o_recv.at[l])
        plane = pl.ds(pl.multiple_of(c * 512, 512), 512)
        remote(ow.at[l, plane], ow.at[l, plane], of_send.at[l], of_recv.at[l], (sp, partner))

    project_source(0)
    ring_step(0)
    project_source(1)
    ring_step(1)
    ring_step(2)
    gains_load.wait()
    q_load.wait()
    await_bytes(qw.at[0], pw_recv.at[0])
    await_bytes(xg.at[0, pl.ds(0, 3)], x_recv.at[0])
    start_queries(0)
    ring_step(3)
    await_queries(0)
    for m in range(1, 4):
        attend(m, 0)
    for m in range(4, 12):
        ring_step(m)
        if m == 7:
            forward_out(0)
        if m == 10:
            forward_out(1)
        attend(m, 0)
    send_context(0)
    ring_step(12)
    ring_step(13)
    for copy in late:
        copy.wait()
    for i, buf in enumerate((gw, uw, dw)):
        await_bytes(buf.at[0], pw_recv.at[1 + i])
    await_bytes(ow.at[0, pl.ds(0, 512)], of_recv.at[0])
    after_context(0)
    ring_step(14)
    ring_step(15)
    own = after_sum(0)
    xg[1, x] = own
    for k in (2, 1, 3):
        remote(xg.at[1, x], xg.at[1, x], x_send.at[1], x_recv.at[1], (sp, other_x(k) * 2 + c))
    ring_step(16)
    ring_step(17)
    await_bytes(xg.at[1, pl.ds(0, 3)], x_recv.at[1])
    start_queries(1)
    ring_step(18)
    await_queries(1)
    for m in range(9, 19):
        attend(m, 1)
    ring_step(19)
    attend(19, 1)
    send_context(1)
    await_bytes(ow.at[1, pl.ds(0, 512)], of_recv.at[1])
    after_context(1)
    out[...] = after_sum(1)

    for l in range(LAYERS):
        await_bytes(kv.at[l, pl.ds(0, 63)], kvs.at[l])
        await_bytes(xg.at[l, pl.ds(0, 3)], x_send.at[l])
        await_bytes(qsend.at[l], q_send.at[l])
        await_bytes(cx.at[l, pl.ds(0, 7)], c_send.at[l])
        await_bytes(rs.at[l, pl.ds(0, 3)], s_send.at[l])
        await_bytes(ow.at[l, pl.ds(0, 3 * HD)], o_send.at[l])
        await_bytes(ow.at[l, pl.ds(0, 512)], of_send.at[l])
    for i, buf in enumerate((qw, gw, uw, dw)):
        await_bytes(buf.at[0], pw_send.at[i])


def per_device(*args):
    ff = args[8].shape[2]
    hbm = pl.BlockSpec(memory_space=pl.ANY)
    vmem = pltpu.VMEM
    dma = pltpu.SemaphoreType.DMA
    scratch = [
        vmem((128, D), BF),
        vmem((LAYERS, 4, D), BF),
        vmem((LAYERS, D), BF),
        vmem((LAYERS, D, HD), BF),
        vmem((LAYERS, D, HD), BF),
        vmem((2, LAYERS, D, HD), BF),
        vmem((2, LAYERS, D, ff), BF),
        vmem((2, LAYERS, D, ff), BF),
        vmem((2, LAYERS, ff, D), BF),
        vmem((LAYERS, D, D), BF),
        vmem((LAYERS, BLOCKS, 2, HD, HD), BF),
        vmem((LAYERS, 4, ROWS, D), BF),
        vmem((LAYERS, HD, GROUP), BF),
        vmem((LAYERS, HD, GROUP), BF),
        vmem((LAYERS, HD, GROUP), BF),
        vmem((LAYERS, 8, GROUP, HD), BF),
        vmem((LAYERS, 2 * GROUP, HD), BF),
        vmem((LAYERS, GROUP, D), BF),
        vmem((LAYERS, 4, ROWS, D), BF),
        vmem((LAYERS, 4, ROWS, D), BF),
        vmem((1, 2 * GROUP), F32),
        vmem((1, 2 * GROUP), F32),
        vmem((HD, 2 * GROUP), F32),
        dma((STEPS, 4, 2)),
        dma((LAYERS, 4, 2)),
        dma((LAYERS,)),
        dma((7,)),
        dma((3,)),
        dma((LAYERS,)),
    ]
    scratch += [dma((LAYERS,)) for _ in range(8)]
    scratch += [dma((4,)), dma((4,))]
    scratch += [dma((LAYERS,)) for _ in range(4)]
    return pl.pallas_call(
        kernel,
        out_shape=jax.ShapeDtypeStruct((ROWS, D), BF),
        in_specs=[hbm] * 11,
        out_specs=pl.BlockSpec(memory_space=pltpu.VMEM),
        scratch_shapes=scratch,
        compiler_params=pltpu.CompilerParams(
            collective_id=0, has_side_effects=True, vmem_limit_bytes=60 * 1024 * 1024
        ),
    )(*args)


def solution(mesh):
    placed = (
        P(("sp", "tp"), None),
        P("sp", None),
        P(),
        P(),
        P(None, None, "tp"),
        P(None, None, "tp"),
        P(None, None, "tp"),
        P(None, "tp", None),
        P(None, None, "tp"),
        P(None, None, "tp"),
        P(None, "tp", None),
    )
    return jax.shard_map(
        per_device, mesh=mesh, in_specs=placed, out_specs=P(("sp", "tp"), None), check_vma=False
    )
```

time: 268 us -> 113 us (0.42)
  Pallas kernels: 0 us -> 108 us
  blocking collectives: 108 us -> 0 us
  waiting for transfers between devices: 87.5 us -> 0 us
  matrix products: 35.2 us -> 0 us
  other arithmetic: 17.6 us -> 0 us
  between operations: 13.6 us -> 0.01 us
  starting transfers between devices: 4.48 us -> 0 us
  local copies, waits for them, and re-layouts: 1.02 us -> 5.08 us
    all_to_all x7 -> x0, blocking collectives: 108 us -> none  [the longest x4 63.6 us: sent_and_summed(): lax.all_to_all(blocks, axis, split_axis=0, concat_axis=0, tiled=True)]
    pallas_call x0 -> x1, Pallas kernels: none -> 108 us  [per_device(): pl.pallas_call(kernel, out_shape=jax.ShapeDtypeStruct((ROWS, D), BF), in_...]
    all_gather x2 -> x0, waiting for transfers between devices: 87.4 us -> none  [in_one_piece(): result = lax.all_gather(both, axis, axis=dim, tiled=True)]
    dot_general x12 -> x0, matrix products: 35.2 us -> none  [the longest x2 13.2 us: attend(): jnp.einsum('thd,shd->ths', query_heads, key_heads, preferred_element_type...]
    reduce_sum x15 -> x0, other arithmetic: 12.6 us -> none  [the longest x2 9.1 us: attend(): running_sum = jnp.sum(weights, axis=-1)]
    unnamed x8 -> x5, local copies, waits for them, and re-layouts: 0.02 us -> 5.08 us
    all_to_all x1 -> x0, starting transfers between devices: 4.44 us -> none  [sent_to_all(): return lax.all_to_all(copies, axis, split_axis=0, concat_axis=0, tiled=True)]
    convert_element_type x6 -> x0, other arithmetic: 2.85 us -> none  [the longest x2 1.02 us: per_device(): normed = rms_norm(stream, layer_gains[0]).astype(jnp.bfloat16)]
  transfers between devices with their start and end apart: 3 -> 0, of which waited for: 2 -> 0; matrix products, arithmetic and copies ran while one was open for 10% -> 0% of each run, Pallas kernels for 0% -> 0%
where the time goes in v1:
time: 113 us
  Pallas kernels  108 us (96%)
  local copies, waits for them, and re-layouts  5.08 us (4%)
    pallas_call x1, Pallas kernels, per_device(): pl.pallas_call(kernel, out_shape=jax.ShapeDtypeStruct((ROWS, D), BF), in_...  108 us
    unnamed x5, local copies, waits for them, and re-layouts  5.08 us

profile of v1, /device:TPU:1, one launch (start us, length us, event | category | flops | bytes accessed | tf_op | source)
XLA Modules:
  0.0 112.6 jit_solution(4334345670247094701)
XLA Ops:
  0.0 0.0 copy-start
  0.0 2.3 %copy.12.gw_in = bf16[2,1024,192]{2,1,0:T(8,128)(2,1)} copy(bf16[2,1024,192]{1,2,0:T(8,128)(2,1)} %param.19) | data formatting | bytes 1572864 | tf_op args[8]
  2.3 0.0 copy-done
  2.3 1.3 %copy.13.uw_in = bf16[2,1024,192]{2,1,0:T(8,128)(2,1)} copy(bf16[2,1024,192]{1,2,0:T(8,128)(2,1)S(1)} %copy-done) | data formatting | bytes 1572864 | tf_op args[9]
  3.6 107.5 %shard_map.109 = bf16[32,1024]{1,0:T(8,128)(2,1)} custom-call(bf16[32,1024]{1,0:T(8,128)(2,1)} %target.1, bf16[128,1024]{1,0:T(8,128)(2,1)} %source.1, bf16[2,4,1024]{2,1,0:T(4,128)(2,1)} %tgains.1, bf16[2,1024]{1,0:T(2,128)(2,1)} %sgain.1, bf16[2,1024,128]{2,1,0:T(8,128)(2,1)} %qw_in.1, bf16[2,1024,128]{2,1,0:T(8,128)(2,1)} %kw_in.1, ...), custom_call_target="tpu_custom_call" | custom-call | tf_op jit(solution)/shard_map/pallas_call | solution.py:397
  111.2 1.5 %copy.15 = bf16[32,1024]{1,0:T(8,128)(2,1)} copy(bf16[32,1024]{1,0:T(8,128)(2,1)} %shard_map.109) | data formatting | bytes 131072
Async XLA Ops:
  0.0 2.3 %copy-start = (bf16[2,1024,192]{1,2,0:T(8,128)(2,1)S(1)}, bf16[2,1024,192]{1,2,0:T(8,128)(2,1)}, u32[]{:S(2)}) copy-start(bf16[2,1024,192]{1,2,0:T(8,128)(2,1)} %param.20) | copy-start | bytes 2359300

commit v2 on v1

--- a/solution.py
+++ b/solution.py
@@ -19,6 +19,8 @@
 BLOCKS = 64
 LAYERS = 2
 STEPS = 8 * LAYERS
+LATENCY = 2.5
+SECOND_START = 25.0
 QSCALE = HD ** (-0.5) * math.log2(math.e)
 
 
@@ -35,12 +37,64 @@
     return ((k + 1) // 2) * (2 * (k % 2) - 1)
 
 
+def ring_events(latency, second_start, block=0.7):
+    queues = {(way, ring): [] for way in (0, 1) for ring in (1, 2)}
+    flying, events = [], []
+    starts = [(0.0, 0), (second_start, 1)]
+    halves = [0, 0]
+    now = 0.0
+
+    def put(ring, index, hop, way):
+        size = block if hop < 4 else block / 2
+        queues[way, ring].append([size, (ring, index, hop, way)])
+
+    def fresh(n):
+        put(2, n, 1, 0)
+        put(2, n, 1, 1)
+
+    while True:
+        times = [t for t, _ in starts] + [t for t, _ in flying]
+        for way in (0, 1):
+            busy = [r for r in (1, 2) if queues[way, r]]
+            times += [now + queues[way, r][0][0] * len(busy) for r in busy]
+        if not times:
+            return events
+        step = min(times) - now
+        for way in (0, 1):
+            busy = [r for r in (1, 2) if queues[way, r]]
+            for r in busy:
+                queues[way, r][0][0] -= step / len(busy)
+        now += step
+        for pair in sorted(queues):
+            if queues[pair] and queues[pair][0][0] < 1e-9:
+                flying.append((now + latency, queues[pair].pop(0)[1]))
+        for start in [v for v in starts if v[0] <= now + 1e-9]:
+            starts.remove(start)
+            events.append((now, (0, start[1], 0, 0)))
+            put(1, start[1], 1, 0)
+            put(1, start[1], 1, 1)
+            fresh(8 * start[1])
+        for arrival in [v for v in flying if v[0] <= now + 1e-9]:
+            flying.remove(arrival)
+            events.append((now, arrival[1]))
+            ring, index, hop, way = arrival[1]
+            if hop < 4:
+                put(ring, index, hop + 1, way)
+            if ring == 1:
+                if hop < 4:
+                    fresh(8 * index + 2 * hop - way)
+                else:
+                    halves[index] += 1
+                    if halves[index] == 2:
+                        fresh(8 * index + 7)
+
+
 def kernel(
     target, source, tgains, sgain, qw_in, kw_in, vw_in, ow_in, gw_in, uw_in, dw_in,
     out,
-    src_v, tg_v, sg_v, kw, vw, qw, gw, uw, dw, ow,
+    src_v, tg_v, sg_v, kw, vw, qw, gu, dn, ow,
     kv, xg, qown, qrecv, qsend, cx, csend, mid, rsend, rs,
-    m_ref, l_ref, acc_ref,
+    m_ref, l_ref, acc_ref, scores_ref,
     r2, r1, kvs, loc, wts, own_sem, x_recv, x_send, q_recv, q_send, c_recv, c_send, s_recv, s_send,
     pw_recv, pw_send, o_recv, o_send, of_recv, of_send,
 ):
@@ -79,23 +133,20 @@
     target_load = local(target, xg.at[0, x], loc.at[4])
     gains_load = local(tgains, tg_v, loc.at[5])
     q_load = local(qw_in, qw.at[c], loc.at[6])
+    ff = dw_in.shape[1]
+    gate_part = gu.at[:, pl.ds(pl.multiple_of(c * 2 * ff, 2 * ff), ff)]
+    up_part = gu.at[:, pl.ds(pl.multiple_of(c * 2 * ff + ff, ff), ff)]
+    down_part = dn.at[:, pl.ds(pl.multiple_of(c * ff, ff), ff)]
     late = [
-        local(gw_in, gw.at[c], wts.at[0]),
-        local(uw_in, uw.at[c], wts.at[1]),
-        local(dw_in, dw.at[c], wts.at[2]),
+        local(gw_in, gate_part, wts.at[0]),
+        local(uw_in, up_part, wts.at[1]),
+        local(dw_in, down_part, wts.at[2]),
     ]
     own_rows = pl.ds(pl.multiple_of((c * 4 + x) * HD, HD), HD)
     own_out = [
         local(ow_in.at[l], ow.at[l, own_rows], own_sem.at[l]) for l in range(LAYERS)
     ]
 
-    barrier = pltpu.get_barrier_semaphore()
-    peers = [(ring1[0], tp), (ring1[1], tp), (ring2[0], tp), (ring2[1], tp)]
-    peers += [(sp, lax.rem(tp + k, 8)) for k in range(1, 8)]
-    for peer in peers:
-        pl.semaphore_signal(barrier, inc=1, device_id=peer, device_id_type=MESH)
-    pl.semaphore_wait(barrier, len(peers))
-
     def remote(src, dst, send, recv, device):
         pltpu.make_async_remote_copy(
             src_ref=src, dst_ref=dst, send_sem=send, recv_sem=recv,
@@ -104,18 +155,6 @@
 
     def await_bytes(ref, sem):
         pltpu.make_async_copy(ref, ref, sem).wait()
-
-    target_load.wait()
-    for k in (2, 1, 3):
-        remote(xg.at[0, x], xg.at[0, x], x_send.at[0], x_recv.at[0], (sp, other_x(k) * 2 + c))
-    for i, (w_in, buf) in enumerate(((qw_in, qw), (gw_in, gw), (uw_in, uw), (dw_in, dw))):
-        remote(w_in, buf.at[c], pw_send.at[i], pw_recv.at[i], (sp, partner))
-    for l in range(LAYERS):
-        for k in (2, 1, 3):
-            remote(
-                ow_in.at[l], ow.at[l, own_rows], o_send.at[l], o_recv.at[l],
-                (sp, other_x(k) * 2 + c),
-            )
 
     def slot_of(fp, spos):
         return fp * 8 + spos
@@ -165,53 +204,63 @@
             block = block.at[way]
         await_bytes(block, r2.at[n, hop - 1, way])
 
-    def ring_step(m):
-        for l in range(LAYERS):
-            hop = m - 4 * l
-            if hop == 0:
-                for way in (0, 1):
-                    send1(l, 1, way)
-            elif 1 <= hop <= 4:
-                for way in (1, 0):
-                    recv1(l, hop, way)
-                    if hop < 4:
-                        send1(l, hop + 1, way)
-        if m < STEPS:
-            for way in (0, 1):
-                send2(m, 1, way)
-        for hop in (1, 2, 3, 4):
-            n = m - hop
-            if 0 <= n < STEPS:
-                for way in (0, 1):
-                    recv2(n, hop, way)
-                    if hop < 4:
-                        send2(n, hop + 1, way)
-
-    def attend(m, l):
-        low = max(1, m - (8 * l + 7))
-        high = min(4, m - 8 * l)
-        if low > high:
+    halves = {}
+    waiting = []
+
+    def handle(event):
+        ring, index, hop, way = event
+        if ring == 0:
+            for w in (0, 1):
+                send1(index, 1, w)
+            for w in (0, 1):
+                send2(8 * index, 1, w)
+            waiting.append((index, 0, 0))
             return
-
-        def body(hop, carry):
-            k = m - hop - 8 * l
-            fp = wrap(f + ring_offset(k))
-            left = slot_of(fp, wrap(s - lax.rem(hop, 4)))
-            right = slot_of(fp, wrap(s + hop))
-            queries = qcat(l)
-            key_pair = jnp.concatenate([kv[l, left, 0], kv[l, right, 0]], axis=0)
-            value_pair = jnp.concatenate([kv[l, left, 1], kv[l, right, 1]], axis=1)
-            scores = dot(key_pair, queries)
-            old = m_ref[...]
-            new = jnp.maximum(old, jnp.max(scores, axis=0, keepdims=True))
-            shrink = jnp.exp2(old - new)
-            weights = jnp.exp2(scores - new)
-            m_ref[...] = new
-            l_ref[...] = l_ref[...] * shrink + jnp.sum(weights, axis=0, keepdims=True)
-            acc_ref[...] = acc_ref[...] * shrink + dot(value_pair, weights.astype(BF))
-            return carry
-
-        lax.fori_loop(low, high + 1, body, 0)
+        if hop == 4:
+            halves[ring, index] = halves.get((ring, index), 0) + 1
+        whole = hop < 4 or halves[ring, index] == 2
+        if ring == 1:
+            k = 2 * hop - way if hop < 4 else 7
+            recv1(index, hop, way)
+            if hop < 4:
+                send1(index, hop + 1, way)
+            if whole:
+                for w in (0, 1):
+                    send2(8 * index + k, 1, w)
+                waiting.append((index, k, 0))
+        else:
+            recv2(index, hop, way)
+            if hop < 4:
+                send2(index, hop + 1, way)
+            if whole:
+                waiting.append((index // 8, index % 8, -hop if way == 0 else hop))
+
+    groups = {0: [], 1: []}
+
+    def attend(l, slots):
+        done = groups[l]
+        if slots is not None:
+            keys = jnp.concatenate([kv[l, slot, 0] for slot in slots], axis=0)
+            scores_ref[len(done) % 2] = dot(keys, qcat(l))
+            done.append(slots)
+        if len(done) == 1 and slots is not None:
+            return
+        past = -2 if slots is not None else -1
+        values = jnp.concatenate([kv[l, slot, 1] for slot in done[past]], axis=1)
+        scores = scores_ref[(len(done) + past) % 2]
+        old = m_ref[...]
+        new = jnp.maximum(old, jnp.max(scores, axis=0, keepdims=True))
+        shrink = jnp.exp2(old - new)
+        weights = jnp.exp2(scores - new)
+        m_ref[...] = new
+        l_ref[...] = l_ref[...] * shrink + jnp.sum(weights, axis=0, keepdims=True)
+        acc_ref[...] = acc_ref[...] * shrink + dot(values, weights.astype(BF))
+
+    def attend_waiting(l):
+        blocks = [v for v in waiting if v[0] == l][:8]
+        for v in blocks:
+            waiting.remove(v)
+        attend(l, [slot_of(wrap(f + ring_offset(k)), wrap(s + d)) for _, k, d in blocks])
 
     def qcat(l):
         return jnp.concatenate([qown[l], qrecv[l]], axis=1)
@@ -251,7 +300,7 @@
         )
         cx[l, slot] = context[:GROUP]
 
-    def after_context(l):
+    def after_context(l, between=None):
         await_bytes(cx.at[l, pl.ds(0, 7)], c_recv.at[l])
         gains = tg_v[l].astype(F32)
         contexts = jnp.concatenate([cx[l, j] for j in range(8)], axis=1)
@@ -259,14 +308,19 @@
         rows = xg[l].reshape(GROUP, D).astype(F32)
         stream = (rows + rms(attended, gains[1:2])).astype(BF)
         mid[l] = stream
-        mixer_in = rms(stream.astype(F32), gains[2:3]).astype(BF)
-        mixed = None
+        if between is not None:
+            between()
+        mixer_in = rms(mid[l].astype(F32), gains[2:3]).astype(BF)
+        both = lax.dot_general(
+            gu[l], mixer_in, (((1,), (1,)), ((), ())), preferred_element_type=F32
+        )
+        parts = []
         for j in range(2):
-            gate = dot(mixer_in, gw[j, l])
-            up = dot(mixer_in, uw[j, l])
-            hidden = (gate / (1.0 + jnp.exp(-gate)) * up).astype(BF)
-            term = dot(hidden, dw[j, l])
-            mixed = term if mixed is None else mixed + term
+            gate = both[2 * j * ff : (2 * j + 1) * ff]
+            up = both[(2 * j + 1) * ff : (2 * j + 2) * ff]
+            parts.append(gate / (1.0 + jnp.exp(-gate)) * up)
+        hidden = jnp.transpose(jnp.concatenate(parts, axis=0)).astype(BF)
+        mixed = dot(hidden, dn[l])
         rsend[l] = mixed.astype(BF).reshape(4, ROWS, D)
         for k in (2, 1, 3):
             remote(
@@ -283,61 +337,92 @@
             total = total + rs[l, j].astype(F32)
         mixer_out = total.astype(BF).astype(F32)
         own = mid[l, pl.ds(pl.multiple_of(x * ROWS, ROWS), ROWS)].astype(F32)
-        return (own + rms(mixer_out, gain)).astype(BF)
+        return own + rms(mixer_out, gain)
 
     def forward_out(l):
-        for k in range(1):
-            own_out[l].wait()
+        own_out[l].wait()
         await_bytes(ow.at[l, pl.ds(0, 3 * HD)], o_recv.at[l])
         plane = pl.ds(pl.multiple_of(c * 512, 512), 512)
         remote(ow.at[l, plane], ow.at[l, plane], of_send.at[l], of_recv.at[l], (sp, partner))
 
+    def send_target():
+        target_load.wait()
+        for k in (2, 1, 3):
+            remote(xg.at[0, x], xg.at[0, x], x_send.at[0], x_recv.at[0], (sp, other_x(k) * 2 + c))
+        remote(qw_in, qw.at[c], pw_send.at[0], pw_recv.at[0], (sp, partner))
+
+    def send_out(l):
+        for k in (2, 1, 3):
+            remote(
+                ow_in.at[l], ow.at[l, own_rows], o_send.at[l], o_recv.at[l],
+                (sp, other_x(k) * 2 + c),
+            )
+
+    def send_ff():
+        for i, (w_in, part) in enumerate(((gw_in, gate_part), (uw_in, up_part), (dw_in, down_part))):
+            remote(w_in, part, pw_send.at[1 + i], pw_recv.at[1 + i], (sp, partner))
+
     project_source(0)
-    ring_step(0)
+    barrier = pltpu.get_barrier_semaphore()
+    peers = [(ring1[0], tp), (ring1[1], tp), (ring2[0], tp), (ring2[1], tp)]
+    peers += [(sp, lax.rem(tp + k, 8)) for k in range(1, 8)]
+    for peer in peers:
+        pl.semaphore_signal(barrier, inc=1, device_id=peer, device_id_type=MESH)
+    pl.semaphore_wait(barrier, len(peers))
+
+    events = ring_events(LATENCY, SECOND_START)
+    last_first = max(t for t, (r, i, _, _) in events if i < (8 if r == 2 else 1))
+    hooks = {}
+
+    def run_until(limit, attending):
+        while events and events[0][0] <= limit:
+            when, event = events.pop(0)
+            for hook_time in sorted(hooks):
+                if hook_time <= when:
+                    hooks.pop(hook_time)()
+            handle(event)
+            if attending is not None and sum(v[0] == attending for v in waiting) >= 8:
+                attend_waiting(attending)
+
+    hooks[20.0] = lambda: forward_out(0)
+    hooks[29.0] = lambda: forward_out(1)
+    run_until(0.0, None)
+    send_target()
     project_source(1)
-    ring_step(1)
-    ring_step(2)
+    send_out(0)
+    run_until(6.0, None)
+    send_out(1)
     gains_load.wait()
     q_load.wait()
     await_bytes(qw.at[0], pw_recv.at[0])
     await_bytes(xg.at[0, pl.ds(0, 3)], x_recv.at[0])
     start_queries(0)
-    ring_step(3)
+    run_until(9.0, None)
+    send_ff()
     await_queries(0)
-    for m in range(1, 4):
-        attend(m, 0)
-    for m in range(4, 12):
-        ring_step(m)
-        if m == 7:
-            forward_out(0)
-        if m == 10:
-            forward_out(1)
-        attend(m, 0)
+    run_until(last_first, 0)
+    attend(0, None)
     send_context(0)
-    ring_step(12)
-    ring_step(13)
+    run_until(last_first + 6.5, None)
     for copy in late:
         copy.wait()
-    for i, buf in enumerate((gw, uw, dw)):
-        await_bytes(buf.at[0], pw_recv.at[1 + i])
+    for i, part in enumerate((gate_part, up_part, down_part)):
+        await_bytes(part, pw_recv.at[1 + i])
     await_bytes(ow.at[0, pl.ds(0, 512)], of_recv.at[0])
-    after_context(0)
-    ring_step(14)
-    ring_step(15)
-    own = after_sum(0)
-    xg[1, x] = own
+    after_context(0, lambda: run_until(last_first + 7.7, None))
+    run_until(last_first + 13.5, None)
+    xg[1, x] = after_sum(0).astype(BF)
     for k in (2, 1, 3):
         remote(xg.at[1, x], xg.at[1, x], x_send.at[1], x_recv.at[1], (sp, other_x(k) * 2 + c))
-    ring_step(16)
-    ring_step(17)
+    run_until(last_first + 18.5, None)
     await_bytes(xg.at[1, pl.ds(0, 3)], x_recv.at[1])
     start_queries(1)
-    ring_step(18)
+    run_until(last_first + 20.5, None)
     await_queries(1)
-    for m in range(9, 19):
-        attend(m, 1)
-    ring_step(19)
-    attend(19, 1)
+    while sum(v[0] == 1 for v in waiting) >= 8:
+        attend_waiting(1)
+    run_until(1000.0, 1)
+    attend(1, None)
     send_context(1)
     await_bytes(ow.at[1, pl.ds(0, 512)], of_recv.at[1])
     after_context(1)
@@ -351,12 +436,16 @@
         await_bytes(rs.at[l, pl.ds(0, 3)], s_send.at[l])
         await_bytes(ow.at[l, pl.ds(0, 3 * HD)], o_send.at[l])
         await_bytes(ow.at[l, pl.ds(0, 512)], of_send.at[l])
-    for i, buf in enumerate((qw, gw, uw, dw)):
-        await_bytes(buf.at[0], pw_send.at[i])
+    await_bytes(qw.at[0], pw_send.at[0])
+    for i, part in enumerate((gate_part, up_part, down_part)):
+        await_bytes(part, pw_send.at[1 + i])
 
 
 def per_device(*args):
+    args = list(args)
     ff = args[8].shape[2]
+    args[8] = jnp.swapaxes(args[8], 1, 2)
+    args[9] = jnp.swapaxes(args[9], 1, 2)
     hbm = pl.BlockSpec(memory_space=pl.ANY)
     vmem = pltpu.VMEM
     dma = pltpu.SemaphoreType.DMA
@@ -367,9 +456,8 @@
         vmem((LAYERS, D, HD), BF),
         vmem((LAYERS, D, HD), BF),
         vmem((2, LAYERS, D, HD), BF),
-        vmem((2, LAYERS, D, ff), BF),
-        vmem((2, LAYERS, D, ff), BF),
-        vmem((2, LAYERS, ff, D), BF),
+        vmem((LAYERS, 4 * ff, D), BF),
+        vmem((LAYERS, 2 * ff, D), BF),
         vmem((LAYERS, D, D), BF),
         vmem((LAYERS, BLOCKS, 2, HD, HD), BF),
         vmem((LAYERS, 4, ROWS, D), BF),
@@ -384,6 +472,7 @@
         vmem((1, 2 * GROUP), F32),
         vmem((1, 2 * GROUP), F32),
         vmem((HD, 2 * GROUP), F32),
+        vmem((2, 8 * HD, 2 * GROUP), F32),
         dma((STEPS, 4, 2)),
         dma((LAYERS, 4, 2)),
         dma((LAYERS,)),
@@ -394,9 +483,9 @@
     scratch += [dma((LAYERS,)) for _ in range(8)]
     scratch += [dma((4,)), dma((4,))]
     scratch += [dma((LAYERS,)) for _ in range(4)]
-    return pl.pallas_call(
+    wide = pl.pallas_call(
         kernel,
-        out_shape=jax.ShapeDtypeStruct((ROWS, D), BF),
+        out_shape=jax.ShapeDtypeStruct((ROWS, D), F32),
         in_specs=[hbm] * 11,
         out_specs=pl.BlockSpec(memory_space=pltpu.VMEM),
         scratch_shapes=scratch,
@@ -404,6 +493,7 @@
             collective_id=0, has_side_effects=True, vmem_limit_bytes=60 * 1024 * 1024
         ),
     )(*args)
+    return wide.astype(BF)
 
 
 def solution(mesh):

time: 113 us -> 93.7 us (0.83)
  Pallas kernels: 108 us -> 92 us
  local copies, waits for them, and re-layouts: 5.08 us -> 0 us
  other arithmetic: 0 us -> 1.54 us
    pallas_call x1, Pallas kernels: 108 us -> 92 us  [per_device(): pl.pallas_call(kernel, out_shape=jax.ShapeDtypeStruct((ROWS, D), F32), in...]
    unnamed x5 -> x0, local copies, waits for them, and re-layouts: 5.08 us -> none
    convert_element_type x0 -> x1, other arithmetic: none -> 1.54 us  [per_device(): return wide.astype(BF)]
where the time goes in v2:
time: 93.7 us; the launch traced here: 93.6 us
  Pallas kernels  92 us (98%)
  other arithmetic  1.54 us (2%)
    pallas_call x1, Pallas kernels, per_device(): pl.pallas_call(kernel, out_shape=jax.ShapeDtypeStruct((ROWS, D), F32), in...  92 us

profile of v2, /device:TPU:1, one launch (start us, length us, event | category | flops | bytes accessed | tf_op | source)
XLA Modules:
  0.0 93.6 jit_solution(5347414507076562674)
XLA Ops:
  0.0 92.0 %shard_map.109 = f32[32,1024]{1,0:T(8,128)} custom-call(bf16[32,1024]{1,0:T(8,128)(2,1)} %target.1, bf16[128,1024]{1,0:T(8,128)(2,1)} %source.1, bf16[2,4,1024]{2,1,0:T(4,128)(2,1)} %tgains.1, bf16[2,1024]{1,0:T(2,128)(2,1)} %sgain.1, bf16[2,1024,128]{2,1,0:T(8,128)(2,1)} %qw_in.1, bf16[2,1024,128]{2,1,0:T(8,128)(2,1)} %kw_in.1, ...), custom_call_target="tpu_custom_call" | custom-call | tf_op jit(solution)/shard_map/pallas_call | solution.py:486
  92.0 1.5 %convert_element_type.3 = bf16[32,1024]{1,0:T(8,128)(2,1)} convert(f32[32,1024]{1,0:T(8,128)} %shard_map.109) | non-fusion elementwise | flops 32768 | bytes 196608 | tf_op jit(solution)/shard_map/convert_element_type | solution.py:496

commit v3 on v2

--- a/solution.py
+++ b/solution.py
@@ -16,11 +16,15 @@
 D = 1024
 ROWS = 32
 GROUP = 128
+HALF = ROWS // 2
+PART = GROUP // 2
 BLOCKS = 64
 LAYERS = 2
 STEPS = 8 * LAYERS
 LATENCY = 2.5
-SECOND_START = 25.0
+SECOND_START = 1.0
+RELEASES = [26.0 + 1.4 * j for j in range(8)]
+MARKS = (3.5, 5.0, 9.0, 14.0, 15.5)
 QSCALE = HD ** (-0.5) * math.log2(math.e)
 
 
@@ -37,11 +41,13 @@
     return ((k + 1) // 2) * (2 * (k % 2) - 1)
 
 
-def ring_events(latency, second_start, block=0.7):
+def ring_events(latency, second_start, releases, block=0.7):
     queues = {(way, ring): [] for way in (0, 1) for ring in (1, 2)}
     flying, events = [], []
-    starts = [(0.0, 0), (second_start, 1)]
+    starts = [(0.0, (0, 0, 0, 0)), (second_start, (0, 1, 0, 0))]
+    starts += [(t, (3, 8 + j, 0, 0)) for j, t in enumerate(releases)]
     halves = [0, 0]
+    here, released = set(), set()
     now = 0.0
 
     def put(ring, index, hop, way):
@@ -49,8 +55,13 @@
         queues[way, ring].append([size, (ring, index, hop, way)])
 
     def fresh(n):
-        put(2, n, 1, 0)
-        put(2, n, 1, 1)
+        if n < 8 or (n in here and n in released):
+            put(2, n, 1, 0)
+            put(2, n, 1, 1)
+
+    def arrived(n):
+        here.add(n)
+        fresh(n)
 
     while True:
         times = [t for t, _ in starts] + [t for t, _ in flying]
@@ -70,10 +81,15 @@
                 flying.append((now + latency, queues[pair].pop(0)[1]))
         for start in [v for v in starts if v[0] <= now + 1e-9]:
             starts.remove(start)
-            events.append((now, (0, start[1], 0, 0)))
-            put(1, start[1], 1, 0)
-            put(1, start[1], 1, 1)
-            fresh(8 * start[1])
+            events.append((now, start[1]))
+            kind, index, _, _ = start[1]
+            if kind == 0:
+                put(1, index, 1, 0)
+                put(1, index, 1, 1)
+                arrived(8 * index)
+            else:
+                released.add(index)
+                fresh(index)
         for arrival in [v for v in flying if v[0] <= now + 1e-9]:
             flying.remove(arrival)
             events.append((now, arrival[1]))
@@ -82,17 +98,17 @@
                 put(ring, index, hop + 1, way)
             if ring == 1:
                 if hop < 4:
-                    fresh(8 * index + 2 * hop - way)
+                    arrived(8 * index + 2 * hop - way)
                 else:
                     halves[index] += 1
                     if halves[index] == 2:
-                        fresh(8 * index + 7)
+                        arrived(8 * index + 7)
 
 
 def kernel(
     target, source, tgains, sgain, qw_in, kw_in, vw_in, ow_in, gw_in, uw_in, dw_in,
     out,
-    src_v, tg_v, sg_v, kw, vw, qw, gu, dn, ow,
+    src_v, tg_v, sg_v, kw, vw, qw, raw, gu, dn, ow,
     kv, xg, qown, qrecv, qsend, cx, csend, mid, rsend, rs,
     m_ref, l_ref, acc_ref, scores_ref,
     r2, r1, kvs, loc, wts, own_sem, x_recv, x_send, q_recv, q_send, c_recv, c_send, s_recv, s_send,
@@ -124,43 +140,49 @@
         copy.start()
         return copy
 
+    barrier = pltpu.get_barrier_semaphore()
+    peers = [(ring1[0], tp), (ring1[1], tp), (ring2[0], tp), (ring2[1], tp)]
+    peers += [(sp, lax.rem(tp + k, 8)) for k in range(1, 8)]
+    for peer in peers:
+        pl.semaphore_signal(barrier, inc=1, device_id=peer, device_id_type=MESH)
+
     first = [
         local(source, src_v, loc.at[0]),
-        local(kw_in, kw, loc.at[1]),
-        local(vw_in, vw, loc.at[2]),
+        local(kw_in.at[0], kw.at[0], loc.at[1]),
+        local(vw_in.at[0], vw.at[0], loc.at[2]),
         local(sgain, sg_v, loc.at[3]),
     ]
-    target_load = local(target, xg.at[0, x], loc.at[4])
+    target_load = [
+        local(target.at[pl.ds(HALF * h, HALF)], xg.at[0, h, x], loc.at[(4, 9)[h]]) for h in (0, 1)
+    ]
+    def remote(src, dst, send, recv, device):
+        pltpu.make_async_remote_copy(
+            src_ref=src, dst_ref=dst, send_sem=send, recv_sem=recv,
+            device_id=device, device_id_type=MESH,
+        ).start()
+
+    def await_bytes(ref, sem):
+        pltpu.make_async_copy(ref, ref, sem).wait()
+
+    def slot_of(fp, spos):
+        return fp * 8 + spos
+
+    for copy in first:
+        copy.wait()
+    second = [local(kw_in.at[1], kw.at[1], loc.at[7]), local(vw_in.at[1], vw.at[1], loc.at[8])]
     gains_load = local(tgains, tg_v, loc.at[5])
     q_load = local(qw_in, qw.at[c], loc.at[6])
     ff = dw_in.shape[1]
-    gate_part = gu.at[:, pl.ds(pl.multiple_of(c * 2 * ff, 2 * ff), ff)]
-    up_part = gu.at[:, pl.ds(pl.multiple_of(c * 2 * ff + ff, ff), ff)]
-    down_part = dn.at[:, pl.ds(pl.multiple_of(c * ff, ff), ff)]
     late = [
-        local(gw_in, gate_part, wts.at[0]),
-        local(uw_in, up_part, wts.at[1]),
-        local(dw_in, down_part, wts.at[2]),
+        local(gw_in, raw.at[:, pl.ds(0, ff)], wts.at[0]),
+        local(uw_in, raw.at[:, pl.ds(ff, ff)], wts.at[1]),
+        local(dw_in, dn.at[c], wts.at[2]),
     ]
     own_rows = pl.ds(pl.multiple_of((c * 4 + x) * HD, HD), HD)
     own_out = [
         local(ow_in.at[l], ow.at[l, own_rows], own_sem.at[l]) for l in range(LAYERS)
     ]
 
-    def remote(src, dst, send, recv, device):
-        pltpu.make_async_remote_copy(
-            src_ref=src, dst_ref=dst, send_sem=send, recv_sem=recv,
-            device_id=device, device_id_type=MESH,
-        ).start()
-
-    def await_bytes(ref, sem):
-        pltpu.make_async_copy(ref, ref, sem).wait()
-
-    def slot_of(fp, spos):
-        return fp * 8 + spos
-
-    for copy in first:
-        copy.wait()
     wide = src_v[...].astype(F32)
     scaled = wide * lax.rsqrt(jnp.mean(wide * wide, axis=-1, keepdims=True) + EPS)
     source_gains = sg_v[...].astype(F32)
@@ -207,27 +229,38 @@
     halves = {}
     waiting = []
 
+    here, released = set(), set()
+
+    def fresh(n):
+        if n < 8 or (n in here and n in released):
+            for w in (0, 1):
+                send2(n, 1, w)
+
+    def arrived(n):
+        here.add(n)
+        waiting.append((n // 8, n % 8, 0))
+        fresh(n)
+
     def handle(event):
         ring, index, hop, way = event
+        if ring == 3:
+            released.add(index)
+            fresh(index)
+            return
         if ring == 0:
             for w in (0, 1):
                 send1(index, 1, w)
-            for w in (0, 1):
-                send2(8 * index, 1, w)
-            waiting.append((index, 0, 0))
+            arrived(8 * index)
             return
         if hop == 4:
             halves[ring, index] = halves.get((ring, index), 0) + 1
         whole = hop < 4 or halves[ring, index] == 2
         if ring == 1:
-            k = 2 * hop - way if hop < 4 else 7
             recv1(index, hop, way)
             if hop < 4:
                 send1(index, hop + 1, way)
             if whole:
-                for w in (0, 1):
-                    send2(8 * index + k, 1, w)
-                waiting.append((index, k, 0))
+                arrived(8 * index + (2 * hop - way if hop < 4 else 7))
         else:
             recv2(index, hop, way)
             if hop < 4:
@@ -285,59 +318,49 @@
         context = jnp.transpose(acc_ref[...] / l_ref[...]).astype(BF)
         slot = c * 4 + x
         csend[l] = context
+        for h in (0, 1):
+            mine = csend.at[l, pl.ds(h * PART, PART)]
+            theirs = csend.at[l, pl.ds(GROUP + h * PART, PART)]
+            here = cx.at[l, h, slot]
+            for k in (2, 1, 3):
+                chip = other_x(k) * 2
+                remote(mine, here, c_send.at[l], c_recv.at[l, h], (sp, chip + c))
+                remote(theirs, here, c_send.at[l], c_recv.at[l, h], (sp, chip + 1 - c))
+            remote(theirs, here, c_send.at[l], c_recv.at[l, h], (sp, partner))
+            cx[l, h, slot] = context[h * PART : (h + 1) * PART]
+
+    def after_context(l, h):
+        await_bytes(cx.at[l, h, pl.ds(0, 7)], c_recv.at[l, h])
+        gains = tg_v[l].astype(F32)
+        contexts = jnp.concatenate([cx[l, h, j] for j in range(8)], axis=1)
+        attended = dot(contexts, ow[l]).astype(BF).astype(F32)
+        rows = xg[l, h].reshape(PART, D).astype(F32)
+        stream = (rows + rms(attended, gains[1:2])).astype(BF)
+        mid[l, h] = stream.reshape(4, HALF, D)
+        mixer_in = rms(stream.astype(F32), gains[2:3]).astype(BF)
+        mixed = None
+        for j in range(2):
+            both = dot(mixer_in, gu[j, l])
+            gate, up = both[:, :ff], both[:, ff:]
+            hidden = (gate / (1.0 + jnp.exp(-gate)) * up).astype(BF)
+            term = dot(hidden, dn[j, l])
+            mixed = term if mixed is None else mixed + term
+        rsend[l, h] = mixed.astype(BF).reshape(4, HALF, D)
         for k in (2, 1, 3):
             remote(
-                csend.at[l, pl.ds(0, GROUP)], cx.at[l, slot], c_send.at[l], c_recv.at[l],
+                rsend.at[l, h, other_x(k)], rs.at[l, h, x], s_send.at[l], s_recv.at[l, h],
                 (sp, other_x(k) * 2 + c),
             )
-            remote(
-                csend.at[l, pl.ds(GROUP, GROUP)], cx.at[l, slot], c_send.at[l], c_recv.at[l],
-                (sp, other_x(k) * 2 + 1 - c),
-            )
-        remote(
-            csend.at[l, pl.ds(GROUP, GROUP)], cx.at[l, slot], c_send.at[l], c_recv.at[l],
-            (sp, partner),
-        )
-        cx[l, slot] = context[:GROUP]
-
-    def after_context(l, between=None):
-        await_bytes(cx.at[l, pl.ds(0, 7)], c_recv.at[l])
-        gains = tg_v[l].astype(F32)
-        contexts = jnp.concatenate([cx[l, j] for j in range(8)], axis=1)
-        attended = dot(contexts, ow[l]).astype(BF).astype(F32)
-        rows = xg[l].reshape(GROUP, D).astype(F32)
-        stream = (rows + rms(attended, gains[1:2])).astype(BF)
-        mid[l] = stream
-        if between is not None:
-            between()
-        mixer_in = rms(mid[l].astype(F32), gains[2:3]).astype(BF)
-        both = lax.dot_general(
-            gu[l], mixer_in, (((1,), (1,)), ((), ())), preferred_element_type=F32
-        )
-        parts = []
-        for j in range(2):
-            gate = both[2 * j * ff : (2 * j + 1) * ff]
-            up = both[(2 * j + 1) * ff : (2 * j + 2) * ff]
-            parts.append(gate / (1.0 + jnp.exp(-gate)) * up)
-        hidden = jnp.transpose(jnp.concatenate(parts, axis=0)).astype(BF)
-        mixed = dot(hidden, dn[l])
-        rsend[l] = mixed.astype(BF).reshape(4, ROWS, D)
-        for k in (2, 1, 3):
-            remote(
-                rsend.at[l, other_x(k)], rs.at[l, x], s_send.at[l], s_recv.at[l],
-                (sp, other_x(k) * 2 + c),
-            )
-        rs[l, x] = rsend[l, x]
-
-    def after_sum(l):
-        await_bytes(rs.at[l, pl.ds(0, 3)], s_recv.at[l])
+        rs[l, h, x] = rsend[l, h, x]
+
+    def after_sum(l, h):
+        await_bytes(rs.at[l, h, pl.ds(0, 3)], s_recv.at[l, h])
         gain = tg_v[l].astype(F32)[3:4]
-        total = rs[l, 0].astype(F32)
+        total = rs[l, h, 0].astype(F32)
         for j in range(1, 4):
-            total = total + rs[l, j].astype(F32)
+            total = total + rs[l, h, j].astype(F32)
         mixer_out = total.astype(BF).astype(F32)
-        own = mid[l, pl.ds(pl.multiple_of(x * ROWS, ROWS), ROWS)].astype(F32)
-        return own + rms(mixer_out, gain)
+        return mid[l, h, x].astype(F32) + rms(mixer_out, gain)
 
     def forward_out(l):
         own_out[l].wait()
@@ -346,9 +369,10 @@
         remote(ow.at[l, plane], ow.at[l, plane], of_send.at[l], of_recv.at[l], (sp, partner))
 
     def send_target():
-        target_load.wait()
+        for copy in target_load:
+            copy.wait()
         for k in (2, 1, 3):
-            remote(xg.at[0, x], xg.at[0, x], x_send.at[0], x_recv.at[0], (sp, other_x(k) * 2 + c))
+            remote(xg.at[0, :, x], xg.at[0, :, x], x_send.at[0], x_recv.at[0], (sp, other_x(k) * 2 + c))
         remote(qw_in, qw.at[c], pw_send.at[0], pw_recv.at[0], (sp, partner))
 
     def send_out(l):
@@ -358,20 +382,21 @@
                 (sp, other_x(k) * 2 + c),
             )
 
+    def turn_ff():
+        for copy in late:
+            copy.wait()
+        for l in range(LAYERS):
+            gu[c, l] = jnp.transpose(raw[l])
+
     def send_ff():
-        for i, (w_in, part) in enumerate(((gw_in, gate_part), (uw_in, up_part), (dw_in, down_part))):
-            remote(w_in, part, pw_send.at[1 + i], pw_recv.at[1 + i], (sp, partner))
+        remote(gu.at[c], gu.at[c], pw_send.at[1], pw_recv.at[1], (sp, partner))
+        remote(dw_in, dn.at[c], pw_send.at[2], pw_recv.at[2], (sp, partner))
 
     project_source(0)
-    barrier = pltpu.get_barrier_semaphore()
-    peers = [(ring1[0], tp), (ring1[1], tp), (ring2[0], tp), (ring2[1], tp)]
-    peers += [(sp, lax.rem(tp + k, 8)) for k in range(1, 8)]
-    for peer in peers:
-        pl.semaphore_signal(barrier, inc=1, device_id=peer, device_id_type=MESH)
     pl.semaphore_wait(barrier, len(peers))
 
-    events = ring_events(LATENCY, SECOND_START)
-    last_first = max(t for t, (r, i, _, _) in events if i < (8 if r == 2 else 1))
+    events = ring_events(LATENCY, SECOND_START, RELEASES)
+    last_first = max(t for t, (r, i, _, _) in events if r in (1, 2) and i < (8 if r == 2 else 1))
     hooks = {}
 
     def run_until(limit, attending):
@@ -388,14 +413,17 @@
     hooks[29.0] = lambda: forward_out(1)
     run_until(0.0, None)
     send_target()
+    for copy in second:
+        copy.wait()
     project_source(1)
     send_out(0)
+    turn_ff()
     run_until(6.0, None)
     send_out(1)
     gains_load.wait()
     q_load.wait()
     await_bytes(qw.at[0], pw_recv.at[0])
-    await_bytes(xg.at[0, pl.ds(0, 3)], x_recv.at[0])
+    await_bytes(xg.at[0, :, pl.ds(0, 3)], x_recv.at[0])
     start_queries(0)
     run_until(9.0, None)
     send_ff()
@@ -403,21 +431,25 @@
     run_until(last_first, 0)
     attend(0, None)
     send_context(0)
-    run_until(last_first + 6.5, None)
-    for copy in late:
-        copy.wait()
-    for i, part in enumerate((gate_part, up_part, down_part)):
-        await_bytes(part, pw_recv.at[1 + i])
+    await_bytes(gu.at[0], pw_recv.at[1])
+    await_bytes(dn.at[0], pw_recv.at[2])
     await_bytes(ow.at[0, pl.ds(0, 512)], of_recv.at[0])
-    after_context(0, lambda: run_until(last_first + 7.7, None))
-    run_until(last_first + 13.5, None)
-    xg[1, x] = after_sum(0).astype(BF)
-    for k in (2, 1, 3):
-        remote(xg.at[1, x], xg.at[1, x], x_send.at[1], x_recv.at[1], (sp, other_x(k) * 2 + c))
-    run_until(last_first + 18.5, None)
-    await_bytes(xg.at[1, pl.ds(0, 3)], x_recv.at[1])
+    run_until(last_first + MARKS[0], None)
+    after_context(0, 0)
+    run_until(last_first + MARKS[1], None)
+    after_context(0, 1)
+    run_until(last_first + MARKS[2], None)
+    for h in (0, 1):
+        xg[1, h, x] = after_sum(0, h).astype(BF)
+        for k in (2, 1, 3):
+            remote(
+                xg.at[1, h, x], xg.at[1, h, x], x_send.at[1], x_recv.at[1],
+                (sp, other_x(k) * 2 + c),
+            )
+    run_until(last_first + MARKS[3], None)
+    await_bytes(xg.at[1, :, pl.ds(0, 3)], x_recv.at[1])
     start_queries(1)
-    run_until(last_first + 20.5, None)
+    run_until(last_first + MARKS[4], None)
     await_queries(1)
     while sum(v[0] == 1 for v in waiting) >= 8:
         attend_waiting(1)
@@ -425,20 +457,22 @@
     attend(1, None)
     send_context(1)
     await_bytes(ow.at[1, pl.ds(0, 512)], of_recv.at[1])
-    after_context(1)
-    out[...] = after_sum(1)
+    after_context(1, 0)
+    after_context(1, 1)
+    for h in (0, 1):
+        out[pl.ds(h * HALF, HALF)] = after_sum(1, h)
 
     for l in range(LAYERS):
         await_bytes(kv.at[l, pl.ds(0, 63)], kvs.at[l])
-        await_bytes(xg.at[l, pl.ds(0, 3)], x_send.at[l])
+        await_bytes(xg.at[l, :, pl.ds(0, 3)], x_send.at[l])
         await_bytes(qsend.at[l], q_send.at[l])
-        await_bytes(cx.at[l, pl.ds(0, 7)], c_send.at[l])
-        await_bytes(rs.at[l, pl.ds(0, 3)], s_send.at[l])
+        await_bytes(cx.at[l, :, pl.ds(0, 7)], c_send.at[l])
+        await_bytes(rs.at[l, :, pl.ds(0, 3)], s_send.at[l])
         await_bytes(ow.at[l, pl.ds(0, 3 * HD)], o_send.at[l])
         await_bytes(ow.at[l, pl.ds(0, 512)], of_send.at[l])
     await_bytes(qw.at[0], pw_send.at[0])
-    for i, part in enumerate((gate_part, up_part, down_part)):
-        await_bytes(part, pw_send.at[1 + i])
+    await_bytes(gu.at[0], pw_send.at[1])
+    await_bytes(dn.at[0], pw_send.at[2])
 
 
 def per_device(*args):
@@ -456,19 +490,20 @@
         vmem((LAYERS, D, HD), BF),
         vmem((LAYERS, D, HD), BF),
         vmem((2, LAYERS, D, HD), BF),
-        vmem((LAYERS, 4 * ff, D), BF),
         vmem((LAYERS, 2 * ff, D), BF),
+        vmem((2, LAYERS, D, 2 * ff), BF),
+        vmem((2, LAYERS, ff, D), BF),
         vmem((LAYERS, D, D), BF),
         vmem((LAYERS, BLOCKS, 2, HD, HD), BF),
-        vmem((LAYERS, 4, ROWS, D), BF),
+        vmem((LAYERS, 2, 4, HALF, D), BF),
         vmem((LAYERS, HD, GROUP), BF),
         vmem((LAYERS, HD, GROUP), BF),
         vmem((LAYERS, HD, GROUP), BF),
-        vmem((LAYERS, 8, GROUP, HD), BF),
+        vmem((LAYERS, 2, 8, PART, HD), BF),
         vmem((LAYERS, 2 * GROUP, HD), BF),
-        vmem((LAYERS, GROUP, D), BF),
-        vmem((LAYERS, 4, ROWS, D), BF),
-        vmem((LAYERS, 4, ROWS, D), BF),
+        vmem((LAYERS, 2, 4, HALF, D), BF),
+        vmem((LAYERS, 2, 4, HALF, D), BF),
+        vmem((LAYERS, 2, 4, HALF, D), BF),
         vmem((1, 2 * GROUP), F32),
         vmem((1, 2 * GROUP), F32),
         vmem((HD, 2 * GROUP), F32),
@@ -476,16 +511,16 @@
         dma((STEPS, 4, 2)),
         dma((LAYERS, 4, 2)),
         dma((LAYERS,)),
-        dma((7,)),
+        dma((10,)),
         dma((3,)),
         dma((LAYERS,)),
     ]
-    scratch += [dma((LAYERS,)) for _ in range(8)]
-    scratch += [dma((4,)), dma((4,))]
+    scratch += [dma((LAYERS,) + more) for more in ((), (), (), (), (2,), (), (2,), ())]
+    scratch += [dma((3,)), dma((3,))]
     scratch += [dma((LAYERS,)) for _ in range(4)]
     wide = pl.pallas_call(
         kernel,
-        out_shape=jax.ShapeDtypeStruct((ROWS, D), F32),
+        out_shape=pltpu.VMEM((ROWS, D), F32),
         in_specs=[hbm] * 11,
         out_specs=pl.BlockSpec(memory_space=pltpu.VMEM),
         scratch_shapes=scratch,

time: 93.7 us -> 86.3 us (0.921)
  Pallas kernels: 92 us -> 85.5 us
    pallas_call x1, Pallas kernels: 92 us -> 85.5 us  [per_device(): pl.pallas_call(kernel, out_shape=pltpu.VMEM((ROWS, D), F32), in_specs=[hb...]
where the time goes in v3:
time: 86.3 us; the launch traced here: 86.2 us
  Pallas kernels  85.5 us (99%)
    pallas_call x1, Pallas kernels, per_device(): pl.pallas_call(kernel, out_shape=pltpu.VMEM((ROWS, D), F32), in_specs=[hb...  85.5 us

profile of v3, /device:TPU:1, one launch (start us, length us, event | category | flops | bytes accessed | tf_op | source)
XLA Modules:
  0.0 86.2 jit_solution(6781061065585237198)
XLA Ops:
  0.0 85.5 %shard_map.109 = f32[32,1024]{1,0:T(8,128)S(1)} custom-call(bf16[32,1024]{1,0:T(8,128)(2,1)} %target.1, bf16[128,1024]{1,0:T(8,128)(2,1)} %source.1, bf16[2,4,1024]{2,1,0:T(4,128)(2,1)} %tgains.1, bf16[2,1024]{1,0:T(2,128)(2,1)} %sgain.1, bf16[2,1024,128]{2,1,0:T(8,128)(2,1)} %qw_in.1, bf16[2,1024,128]{2,1,0:T(8,128)(2,1)} %kw_in.1, ...), custom_call_target="tpu_custom_call" | custom-call | tf_op jit(solution)/shard_map/pallas_call | solution.py:521
  85.5 0.6 convert_element_type.3

commit v4 on v3

--- a/solution.py
+++ b/solution.py
@@ -22,9 +22,9 @@
 LAYERS = 2
 STEPS = 8 * LAYERS
 LATENCY = 2.5
-SECOND_START = 1.0
-RELEASES = [26.0 + 1.4 * j for j in range(8)]
-MARKS = (3.5, 5.0, 9.0, 14.0, 15.5)
+EXCHANGE = 4.2
+SWAP = 1.4
+RELEASES = (26.2, 26.2, 30.3, 29.6, 31.5, 28.7, 29.2, 30.3)
 QSCALE = HD ** (-0.5) * math.log2(math.e)
 
 
@@ -41,18 +41,18 @@
     return ((k + 1) // 2) * (2 * (k % 2) - 1)
 
 
-def ring_events(latency, second_start, releases, block=0.7):
+def plan(latency, exchange, swap, releases, block=0.7, cost=0.03):
     queues = {(way, ring): [] for way in (0, 1) for ring in (1, 2)}
-    flying, events = [], []
-    starts = [(0.0, (0, 0, 0, 0)), (second_start, (0, 1, 0, 0))]
-    starts += [(t, (3, 8 + j, 0, 0)) for j, t in enumerate(releases)]
-    halves = [0, 0]
+    coming = [(0.0, (0, 0, 0, 0)), (1.0, (0, 1, 0, 0)), (6.0, (4, 0, 0, 0))]
+    coming += [(t, (3, 8 + j, 0, 0)) for j, t in enumerate(releases)]
+    ready, order = [], []
     here, released = set(), set()
+    halves = {}
+    blocks, taken, asked = [0, 0], [0, 0], [False, False]
     now = 0.0
 
     def put(ring, index, hop, way):
-        size = block if hop < 4 else block / 2
-        queues[way, ring].append([size, (ring, index, hop, way)])
+        queues[way, ring].append([block if hop < 4 else block / 2, (ring, index, hop, way)])
 
     def fresh(n):
         if n < 8 or (n in here and n in released):
@@ -61,48 +61,82 @@
 
     def arrived(n):
         here.add(n)
+        blocks[n // 8] += 1
         fresh(n)
 
-    while True:
-        times = [t for t, _ in starts] + [t for t, _ in flying]
-        for way in (0, 1):
-            busy = [r for r in (1, 2) if queues[way, r]]
-            times += [now + queues[way, r][0][0] * len(busy) for r in busy]
-        if not times:
-            return events
-        step = min(times) - now
+    def ends():
         for way in (0, 1):
             busy = [r for r in (1, 2) if queues[way, r]]
             for r in busy:
-                queues[way, r][0][0] -= step / len(busy)
-        now += step
-        for pair in sorted(queues):
-            if queues[pair] and queues[pair][0][0] < 1e-9:
-                flying.append((now + latency, queues[pair].pop(0)[1]))
-        for start in [v for v in starts if v[0] <= now + 1e-9]:
-            starts.remove(start)
-            events.append((now, start[1]))
-            kind, index, _, _ = start[1]
-            if kind == 0:
-                put(1, index, 1, 0)
-                put(1, index, 1, 1)
-                arrived(8 * index)
+                yield queues[way, r][0], len(busy)
+
+    def advance(span):
+        nonlocal now
+        end = now + span
+        while now < end - 1e-9:
+            step = min([end - now] + [item[0] * share for item, share in ends()])
+            for item, share in list(ends()):
+                item[0] -= step / share
+            now += step
+            for key in sorted(queues):
+                if queues[key] and queues[key][0][0] < 1e-9:
+                    coming.append((now + latency, queues[key].pop(0)[1]))
+
+    while True:
+        for v in [v for v in coming if v[0] <= now + 1e-9]:
+            coming.remove(v)
+            ready.append((0 if v[1][0] < 4 else 1, v[1]))
+        for l in (0, 1):
+            if asked[l] and blocks[l] - 8 * taken[l] >= 8 and (2, (8, l, 0, 0)) not in ready:
+                ready.append((2, (8, l, 0, 0)))
+        if not ready:
+            times = [v[0] for v in coming] + [now + item[0] * share for item, share in ends()]
+            advance(max(min(times) - now, 1e-6))
+            continue
+        ready.sort(key=lambda v: v[0])
+        task = ready.pop(0)[1]
+        order.append((now, task))
+        kind, index, hop, way = task
+        if kind == 0:
+            put(1, index, 1, 0)
+            put(1, index, 1, 1)
+            arrived(8 * index)
+        elif kind == 3:
+            released.add(index)
+            fresh(index)
+        elif kind in (1, 2):
+            if hop < 4:
+                put(kind, index, hop + 1, way)
             else:
-                released.add(index)
-                fresh(index)
-        for arrival in [v for v in flying if v[0] <= now + 1e-9]:
-            flying.remove(arrival)
-            events.append((now, arrival[1]))
-            ring, index, hop, way = arrival[1]
-            if hop < 4:
-                put(ring, index, hop + 1, way)
-            if ring == 1:
-                if hop < 4:
-                    arrived(8 * index + 2 * hop - way)
-                else:
-                    halves[index] += 1
-                    if halves[index] == 2:
-                        arrived(8 * index + 7)
+                halves[kind, index] = halves.get((kind, index), 0) + 1
+            whole = hop < 4 or halves[kind, index] == 2
+            if whole and kind == 1:
+                arrived(8 * index + (2 * hop - way if hop < 4 else 7))
+            elif whole:
+                blocks[index // 8] += 1
+        elif kind == 4:
+            advance(0.7)
+            coming.append((now + swap, (5, index, 0, 0)))
+        elif kind == 5:
+            asked[index] = True
+        elif kind == 6:
+            advance(1.35)
+            coming.append((now + exchange - 0.6, (7, 0, hop, 0)))
+        elif kind == 7:
+            advance(0.1)
+            if hop == 1:
+                coming.append((now + exchange - 0.3, (4, 1, 0, 0)))
+        elif kind == 8:
+            taken[index] += 1
+            advance(0.45)
+            if taken[index] == 8:
+                order.append((now, (9, index, 0, 0)))
+                advance(0.45)
+                if index == 1:
+                    return order
+                coming.append((now + exchange - 0.6, (6, 0, 0, 0)))
+                coming.append((now + exchange + 0.8, (6, 0, 1, 0)))
+        advance(cost)
 
 
 def kernel(
@@ -395,68 +429,60 @@
     project_source(0)
     pl.semaphore_wait(barrier, len(peers))
 
-    events = ring_events(LATENCY, SECOND_START, RELEASES)
-    last_first = max(t for t, (r, i, _, _) in events if r in (1, 2) and i < (8 if r == 2 else 1))
-    hooks = {}
-
-    def run_until(limit, attending):
-        while events and events[0][0] <= limit:
-            when, event = events.pop(0)
-            for hook_time in sorted(hooks):
-                if hook_time <= when:
-                    hooks.pop(hook_time)()
-            handle(event)
-            if attending is not None and sum(v[0] == attending for v in waiting) >= 8:
-                attend_waiting(attending)
-
-    hooks[20.0] = lambda: forward_out(0)
-    hooks[29.0] = lambda: forward_out(1)
-    run_until(0.0, None)
-    send_target()
-    for copy in second:
-        copy.wait()
-    project_source(1)
-    send_out(0)
-    turn_ff()
-    run_until(6.0, None)
-    send_out(1)
-    gains_load.wait()
-    q_load.wait()
-    await_bytes(qw.at[0], pw_recv.at[0])
-    await_bytes(xg.at[0, :, pl.ds(0, 3)], x_recv.at[0])
-    start_queries(0)
-    run_until(9.0, None)
-    send_ff()
-    await_queries(0)
-    run_until(last_first, 0)
-    attend(0, None)
-    send_context(0)
-    await_bytes(gu.at[0], pw_recv.at[1])
-    await_bytes(dn.at[0], pw_recv.at[2])
-    await_bytes(ow.at[0, pl.ds(0, 512)], of_recv.at[0])
-    run_until(last_first + MARKS[0], None)
-    after_context(0, 0)
-    run_until(last_first + MARKS[1], None)
-    after_context(0, 1)
-    run_until(last_first + MARKS[2], None)
-    for h in (0, 1):
+    def begin_queries(l):
+        if l == 0:
+            gains_load.wait()
+            q_load.wait()
+            await_bytes(qw.at[0], pw_recv.at[0])
+        await_bytes(xg.at[l, :, pl.ds(0, 3)], x_recv.at[l])
+        start_queries(l)
+        if l == 0:
+            send_out(1)
+            send_ff()
+
+    def end_attention(l):
+        attend(l, None)
+        send_context(l)
+        if l == 0:
+            await_bytes(gu.at[0], pw_recv.at[1])
+            await_bytes(dn.at[0], pw_recv.at[2])
+        await_bytes(ow.at[l, pl.ds(0, 512)], of_recv.at[l])
+
+    def next_rows(h):
         xg[1, h, x] = after_sum(0, h).astype(BF)
         for k in (2, 1, 3):
             remote(
                 xg.at[1, h, x], xg.at[1, h, x], x_send.at[1], x_recv.at[1],
                 (sp, other_x(k) * 2 + c),
             )
-    run_until(last_first + MARKS[3], None)
-    await_bytes(xg.at[1, :, pl.ds(0, 3)], x_recv.at[1])
-    start_queries(1)
-    run_until(last_first + MARKS[4], None)
-    await_queries(1)
-    while sum(v[0] == 1 for v in waiting) >= 8:
-        attend_waiting(1)
-    run_until(1000.0, 1)
-    attend(1, None)
-    send_context(1)
-    await_bytes(ow.at[1, pl.ds(0, 512)], of_recv.at[1])
+
+    def after_start():
+        send_target()
+        for copy in second:
+            copy.wait()
+        project_source(1)
+        send_out(0)
+        turn_ff()
+
+    hooks = [(0.01, after_start), (20.0, lambda: forward_out(0)), (29.0, lambda: forward_out(1))]
+    for when, task in plan(LATENCY, EXCHANGE, SWAP, RELEASES):
+        while hooks and hooks[0][0] <= when:
+            hooks.pop(0)[1]()
+        kind, index, hop, _ = task
+        if kind < 4:
+            handle(task)
+        elif kind == 4:
+            begin_queries(index)
+        elif kind == 5:
+            await_queries(index)
+        elif kind == 6:
+            after_context(index, hop)
+        elif kind == 7:
+            next_rows(hop)
+        elif kind == 8:
+            attend_waiting(index)
+        else:
+            end_attention(index)
     after_context(1, 0)
     after_context(1, 1)
     for h in (0, 1):

time: 86.3 us -> 82.6 us (0.957)
  Pallas kernels: 85.5 us -> 81.9 us
    pallas_call x1, Pallas kernels: 85.5 us -> 81.9 us  [per_device(): pl.pallas_call(kernel, out_shape=pltpu.VMEM((ROWS, D), F32), in_specs=[hb...]
where the time goes in v4:
time: 82.6 us; the launch traced here: 82.5 us
  Pallas kernels  81.9 us (99%)
    pallas_call x1, Pallas kernels, per_device(): pl.pallas_call(kernel, out_shape=pltpu.VMEM((ROWS, D), F32), in_specs=[hb...  81.9 us

profile of v4, /device:TPU:1, one launch (start us, length us, event | category | flops | bytes accessed | tf_op | source)
XLA Modules:
  0.0 82.5 jit_solution(720797073496313292)
XLA Ops:
  0.0 81.9 %shard_map.109 = f32[32,1024]{1,0:T(8,128)S(1)} custom-call(bf16[32,1024]{1,0:T(8,128)(2,1)} %target.1, bf16[128,1024]{1,0:T(8,128)(2,1)} %source.1, bf16[2,4,1024]{2,1,0:T(4,128)(2,1)} %tgains.1, bf16[2,1024]{1,0:T(2,128)(2,1)} %sgain.1, bf16[2,1024,128]{2,1,0:T(8,128)(2,1)} %qw_in.1, bf16[2,1024,128]{2,1,0:T(8,128)(2,1)} %kw_in.1, ...), custom_call_target="tpu_custom_call" | custom-call | tf_op jit(solution)/shard_map/pallas_call | solution.py:547
  81.9 0.6 convert_element_type.3

commit v5 on v4

--- a/solution.py
+++ b/solution.py
@@ -43,7 +43,7 @@
 
 def plan(latency, exchange, swap, releases, block=0.7, cost=0.03):
     queues = {(way, ring): [] for way in (0, 1) for ring in (1, 2)}
-    coming = [(0.0, (0, 0, 0, 0)), (1.0, (0, 1, 0, 0)), (6.0, (4, 0, 0, 0))]
+    coming = [(0.0, (0, 0, 0, 0)), (1.0, (0, 1, 0, 0)), (9.0, (4, 0, 0, 0))]
     coming += [(t, (3, 8 + j, 0, 0)) for j, t in enumerate(releases)]
     ready, order = [], []
     here, released = set(), set()
@@ -116,7 +116,7 @@
                 blocks[index // 8] += 1
         elif kind == 4:
             advance(0.7)
-            coming.append((now + swap, (5, index, 0, 0)))
+            coming.append((now + (swap if index else 3.0), (5, index, 0, 0)))
         elif kind == 5:
             asked[index] = True
         elif kind == 6:
@@ -437,7 +437,7 @@
         await_bytes(xg.at[l, :, pl.ds(0, 3)], x_recv.at[l])
         start_queries(l)
         if l == 0:
-            send_out(1)
+            send_out(0)
             send_ff()
 
     def end_attention(l):
@@ -461,10 +461,9 @@
         for copy in second:
             copy.wait()
         project_source(1)
-        send_out(0)
         turn_ff()
 
-    hooks = [(0.01, after_start), (20.0, lambda: forward_out(0)), (29.0, lambda: forward_out(1))]
+    hooks = [(0.01, after_start), (15.0, lambda: send_out(1)), (23.0, lambda: forward_out(0)), (32.0, lambda: forward_out(1))]
     for when, task in plan(LATENCY, EXCHANGE, SWAP, RELEASES):
         while hooks and hooks[0][0] <= when:
             hooks.pop(0)[1]()

time: 82.6 us -> 80.5 us (0.975)
  Pallas kernels: 81.9 us -> 79.7 us
    pallas_call x1, Pallas kernels: 81.9 us -> 79.7 us  [per_device(): pl.pallas_call(kernel, out_shape=pltpu.VMEM((ROWS, D), F32), in_specs=[hb...]
where the time goes in v5:
time: 80.5 us; the launch traced here: 80.3 us
  Pallas kernels  79.7 us (99%)
    pallas_call x1, Pallas kernels, per_device(): pl.pallas_call(kernel, out_shape=pltpu.VMEM((ROWS, D), F32), in_specs=[hb...  79.7 us

profile of v5, /device:TPU:1, one launch (start us, length us, event | category | flops | bytes accessed | tf_op | source)
XLA Modules:
  0.0 80.3 jit_solution(6065417974016601958)
XLA Ops:
  0.0 79.7 %shard_map.109 = f32[32,1024]{1,0:T(8,128)S(1)} custom-call(bf16[32,1024]{1,0:T(8,128)(2,1)} %target.1, bf16[128,1024]{1,0:T(8,128)(2,1)} %source.1, bf16[2,4,1024]{2,1,0:T(4,128)(2,1)} %tgains.1, bf16[2,1024]{1,0:T(2,128)(2,1)} %sgain.1, bf16[2,1024,128]{2,1,0:T(8,128)(2,1)} %qw_in.1, bf16[2,1024,128]{2,1,0:T(8,128)(2,1)} %kw_in.1, ...), custom_call_target="tpu_custom_call" | custom-call | tf_op jit(solution)/shard_map/pallas_call | solution.py:546
  79.7 0.6 convert_element_type.3

commit v6 on v5

--- a/solution.py
+++ b/solution.py
@@ -43,7 +43,7 @@
 
 def plan(latency, exchange, swap, releases, block=0.7, cost=0.03):
     queues = {(way, ring): [] for way in (0, 1) for ring in (1, 2)}
-    coming = [(0.0, (0, 0, 0, 0)), (1.0, (0, 1, 0, 0)), (9.0, (4, 0, 0, 0))]
+    coming = [(0.0, (0, 0, 0, 0)), (1.0, (0, 1, 0, 0)), (8.2, (4, 0, 0, 0))]
     coming += [(t, (3, 8 + j, 0, 0)) for j, t in enumerate(releases)]
     ready, order = [], []
     here, released = set(), set()

time: 80.5 us -> 80.4 us (level)
  no operation moved by 1% of the time
where the time goes in v6:
time: 80.4 us; the launch traced here: 80.2 us
  Pallas kernels  79.6 us (99%)
    pallas_call x1, Pallas kernels, per_device(): pl.pallas_call(kernel, out_shape=pltpu.VMEM((ROWS, D), F32), in_specs=[hb...  79.6 us

profile of v6, /device:TPU:1, one launch (start us, length us, event | category | flops | bytes accessed | tf_op | source)
XLA Modules:
  0.0 80.2 jit_solution(11504001746526057503)
XLA Ops:
  0.0 79.6 %shard_map.109 = f32[32,1024]{1,0:T(8,128)S(1)} custom-call(bf16[32,1024]{1,0:T(8,128)(2,1)} %target.1, bf16[128,1024]{1,0:T(8,128)(2,1)} %source.1, bf16[2,4,1024]{2,1,0:T(4,128)(2,1)} %tgains.1, bf16[2,1024]{1,0:T(2,128)(2,1)} %sgain.1, bf16[2,1024,128]{2,1,0:T(8,128)(2,1)} %qw_in.1, bf16[2,1024,128]{2,1,0:T(8,128)(2,1)} %kw_in.1, ...), custom_call_target="tpu_custom_call" | custom-call | tf_op jit(solution)/shard_map/pallas_call | solution.py:546
  79.6 0.6 convert_element_type.3
